TPU v7x, 32 devices: a whole 2x2x4 slice. The times are simulated.
32 devices in a mesh: ep: 8 (over z, y), tp: 4 (over x, core).
Axes of the slice: x: 2, y: 2, z: 4, core: 2. Of those that a mesh axis runs over, the one named last changes fastest.
Arguments:
- value_in: bfloat16 [4096, 2048], P('ep', 'tp'), may hold values from -400 to 400
- gate_in: bfloat16 [4096, 2048], P('ep', 'tp'), may hold values from -8 to 8
- conv_taps: float32 [31, 2048], P(None, 'tp'), may hold values from -1 to 1
- conv_bias: float32 [2048], P('tp'), may hold values from -3 to 3
- ln_gain: float32 [2048], P('tp'), may hold values from 0.1 to 1.9
- ln_bias: float32 [2048], P('tp'), may hold values from -3 to 3
- out_proj: bfloat16 [2048, 4096], P('tp'), may hold values from -0.125 to 0.125
- tokens_b: bfloat16 [4096, 4096], P('ep'), may hold values from -6 to 6
- norm_gain: float32 [4096], replicated, may hold values from 0.1 to 1.9
- routes: int32 [4096, 2], P(('ep', 'tp')), may hold values from 0 to 7, all different within a row; in each aligned block of 128 rows (0 to 127, 128 to 255, ...) at most 48 rows name the same one
- route_weights: float32 [4096, 2], P(('ep', 'tp')), may hold values from 0.2 to 1.5
- expert_gate: bfloat16 [8, 4096, 1024], P('ep', None, 'tp'), may hold values from -0.09375 to 0.09375
- expert_up: bfloat16 [8, 4096, 1024], P('ep', None, 'tp'), may hold values from -0.09375 to 0.09375
- expert_down: bfloat16 [8, 1024, 4096], P('ep', 'tp'), may hold values from -0.1875 to 0.1875
- shared_gate: bfloat16 [4096, 1024], P(None, 'tp'), may hold values from -0.09375 to 0.09375
- shared_up: bfloat16 [4096, 1024], P(None, 'tp'), may hold values from -0.09375 to 0.09375
- shared_down: bfloat16 [1024, 4096], P('tp'), may hold values from -0.1875 to 0.1875
Outputs:
- mixer_out: bfloat16 [4096, 4096], P(('ep', 'tp'))
- experts_out: bfloat16 [4096, 4096], P(('ep', 'tp'))
Inputs may be any that keep to these rules, and one draw needn't show every extreme that they name: `routes`: each row names 2 different experts. In each aligned block of 128 rows (the rows of one device) no expert is named by more than 48 rows, and in some blocks an expert is named by exactly 48 rows.
All inputs are finite; a program needn't handle non-finite values.
Results may differ from a plain program's by a relative error of at most 0.012.
Values may be sent and summed in bfloat16 or wider, within the bound.
A program may use at most 128 MiB of HBM per device.

v0:
```python
import jax
import jax.numpy as jnp
from jax import lax
from jax.sharding import PartitionSpec as P

EPSILON = 1e-06
COLUMN_CHUNKS = 2


def shifted(x, axis, by):
    devices = lax.axis_size(axis)
    pairs = [(i, i + by) for i in range(devices) if 0 <= i + by < devices]
    return lax.ppermute(x, axis, pairs)


def swapped(x, axis, bit):
    devices = lax.axis_size(axis)
    return lax.ppermute(x, axis, [(i, i ^ bit) for i in range(devices)])


def stages(axis):
    bits, bit = [], 1
    while bit < lax.axis_size(axis):
        bits.append(bit)
        bit *= 2
    return bits


def gathered(x, axis):
    pieces = [x]
    for bit in reversed(stages(axis)):
        pieces = pieces + [swapped(piece, axis, bit) for piece in pieces]
    return pieces


def scattered_product(lhs, weight, axis):
    count = lax.axis_size(axis)
    me = lax.axis_index(axis)
    bits = stages(axis)
    rows = lhs.shape[0] // count
    width = weight.shape[1]
    near = bits[0]
    core = me % 2
    blocks = lhs.reshape(count // 2, 2, rows, lhs.shape[1])
    sent = lax.dynamic_index_in_dim(blocks, 1 - core, 1, keepdims=False).reshape(-1, lhs.shape[1])
    kept = lax.dynamic_index_in_dim(blocks, core, 1, keepdims=False).reshape(-1, lhs.shape[1])
    sent = jnp.dot(sent, weight, preferred_element_type=jnp.float32).astype(jnp.bfloat16)
    arrived = swapped(sent, axis, near)
    kept = jnp.dot(kept, weight, preferred_element_type=jnp.float32).astype(jnp.bfloat16)
    total = (kept, arrived)
    left = count // 2
    for bit in bits[1:]:
        low = (me // bit) % 2
        halves = [part.reshape(left // 2, 2, rows, width) for part in total]
        give = [lax.dynamic_index_in_dim(h, 1 - low, 1, keepdims=False) for h in halves]
        keep = [lax.dynamic_index_in_dim(h, low, 1, keepdims=False) for h in halves]
        give = sum(g.astype(jnp.float32) for g in give).astype(jnp.bfloat16)
        total = tuple(keep) + (swapped(give, axis, bit),)
        left = left // 2
    return sum(part.reshape(rows, width).astype(jnp.float32) for part in total)


def rms_normed(features, gain):
    features = features.astype(jnp.float32)
    return (
        features
        * lax.rsqrt(jnp.mean(features * features, axis=1, keepdims=True) + EPSILON)
        * gain
    ).astype(jnp.bfloat16)


def gated_hidden(rows_in, weight_gate, weight_up):
    return (
        jax.nn.silu(jnp.dot(rows_in, weight_gate, preferred_element_type=jnp.float32))
        * jnp.dot(rows_in, weight_up, preferred_element_type=jnp.float32)
    ).astype(jnp.bfloat16)


def per_device(
    value_in,
    gate_in,
    conv_taps,
    conv_bias,
    ln_gain,
    ln_bias,
    out_proj,
    tokens_b,
    norm_gain,
    routes,
    route_weights,
    expert_gate,
    expert_up,
    expert_down,
    shared_gate,
    shared_up,
    shared_down,
):
    tp_count = lax.axis_size("tp")
    ep_count = lax.axis_size("ep")
    model_width = tokens_b.shape[1]
    rows_own, top_count = routes.shape
    capacity = max(2, 3 * rows_own * top_count // (2 * ep_count))

    gates = gathered(expert_gate[0], "tp")
    ups = gathered(expert_up[0], "tp")
    chunk = model_width // COLUMN_CHUNKS

    own = lax.dynamic_slice_in_dim(tokens_b, lax.axis_index("tp") * rows_own, rows_own, 0)
    own_rows = rms_normed(own, norm_gain)
    by_choice = routes.T
    expert_ids = jnp.arange(ep_count, dtype=jnp.int32)
    names = by_choice[:, None, :] == expert_ids[None, :, None]
    named = jnp.any(names, axis=0)
    row_ids = jnp.arange(rows_own, dtype=jnp.int32)
    before_row = (row_ids[:, None] < row_ids[None, :]).astype(jnp.bfloat16)
    earlier = jnp.dot(
        named.astype(jnp.bfloat16), before_row, preferred_element_type=jnp.float32
    ).astype(jnp.int32)
    slots = jnp.arange(capacity, dtype=jnp.int32)
    placed = earlier[:, None, :] == slots[None, :, None]
    pick = (placed & named[:, None, :]).astype(jnp.bfloat16).reshape(-1, rows_own)
    outbox = jnp.dot(pick, own_rows, preferred_element_type=jnp.float32).astype(jnp.bfloat16)
    arrived = lax.all_to_all(
        outbox.reshape(ep_count, capacity, model_width), "ep", split_axis=0, concat_axis=0, tiled=True
    ).reshape(ep_count * capacity, model_width)

    gated = (value_in.astype(jnp.float32) * jax.nn.sigmoid(gate_in.astype(jnp.float32))).astype(
        jnp.bfloat16
    )
    rim_rows = conv_taps.shape[0] - 1
    length = gated.shape[0]
    before = shifted(gated[length - rim_rows :], "ep", 1)
    padded = jnp.concatenate([before, gated], axis=0).astype(jnp.float32)
    filtered = jnp.zeros(gated.shape, jnp.float32) + conv_bias[None, :]
    for tap_index in range(rim_rows + 1):
        filtered = filtered + conv_taps[tap_index][None, :] * padded[tap_index : tap_index + length]
    normed_b = rms_normed(tokens_b, norm_gain)
    hidden_shared = gated_hidden(normed_b, shared_gate, shared_up)
    shared_rows = scattered_product(hidden_shared, shared_down, "tp").astype(jnp.bfloat16)

    hidden = [gated_hidden(arrived, g, u) for g, u in zip(gates, ups)]
    parts, products = [], []
    for c in range(COLUMN_CHUNKS):
        local = expert_down[0][:, c * chunk : (c + 1) * chunk]
        if products:
            local, _ = lax.optimization_barrier((local, products[-1]))
        pieces = gathered(local, "tp")
        product = sum(
            jnp.dot(h, piece, preferred_element_type=jnp.float32)
            for h, piece in zip(hidden, pieces)
        ).astype(jnp.bfloat16)
        products.append(product)
        parts.append(
            lax.all_to_all(
                product.reshape(ep_count, capacity, chunk),
                "ep",
                split_axis=0,
                concat_axis=0,
                tiled=True,
            ).reshape(ep_count * capacity, chunk)
        )
    row_sum, squares, _ = lax.optimization_barrier(
        (jnp.sum(filtered, axis=1), jnp.sum(filtered * filtered, axis=1), products[0])
    )
    row_sum, squares = lax.psum((row_sum, squares), "tp")
    channel_count = filtered.shape[1] * tp_count
    average = row_sum / channel_count
    variance = squares / channel_count - average * average
    normed_a = (filtered - average[:, None]) * lax.rsqrt(
        variance[:, None] + EPSILON
    ) * ln_gain + ln_bias
    activated = jax.nn.silu(normed_a).astype(jnp.bfloat16)
    mixer_rows = scattered_product(activated, out_proj, "tp").astype(jnp.bfloat16)

    outs = []
    for c, returned in enumerate(parts):
        total = shared_rows[:, c * chunk : (c + 1) * chunk].astype(jnp.float32)
        for k in range(top_count):
            choice = (placed & names[k][:, None, :]).astype(jnp.bfloat16).reshape(-1, rows_own)
            picked = lax.dot_general(
                choice, returned, (((0,), (0,)), ((), ())), preferred_element_type=jnp.float32
            )
            total = total + picked * route_weights[:, k][:, None]
        outs.append(total.astype(jnp.bfloat16))
    return (mixer_rows, jnp.concatenate(outs, axis=1))


def solution(mesh):
    return jax.shard_map(
        per_device,
        mesh=mesh,
        in_specs=(
            P("ep", "tp"),
            P("ep", "tp"),
            P(None, "tp"),
            P("tp"),
            P("tp"),
            P("tp"),
            P("tp", None),
            P("ep", None),
            P(),
            P(("ep", "tp"), None),
            P(("ep", "tp"), None),
            P("ep", None, "tp"),
            P("ep", None, "tp"),
            P("ep", "tp", None),
            P(None, "tp"),
            P(None, "tp"),
            P("tp", None),
        ),
        out_specs=(P(("ep", "tp"), None), P(("ep", "tp"), None)),
        check_vma=False,
    )
```

profile of v0, /device:TPU:12, one launch (start us, length us, event | category | flops | bytes accessed | tf_op | source)
XLA Modules:
  0.0 232.7 jit_solution(6657440936348305720)
XLA Ops:
  0.6 1.6 collective-permute-start.1
  3.0 1.5 fusion.13
  4.5 0.7 iota_compare_fusion.3
  5.5 4.0 %convolution_convert_fusion = bf16[384,4096]{1,0:T(8,128)(2,1)} fusion(pred[384,128]{1,0:T(32,128)(4,1)S(1)} %fusion.68, f32[4096]{0:T(1024)} %param.25, f32[128]{0:T(128)S(1)} %add_rsqrt_fusion.2, bf16[512,4096]{1,0:T(8,128)(2,1)} %param.24, s32[]{:T(128)S(6)} %select_n.46), kind=kOutput, calls=%fused_computation.5 | convolution fusion | flops 406323200 | bytes 4260356 | tf_op jit(solution)/shard_map/dot_general | solution.py:122
  9.5 6.4 %all-to-all-start = ((bf16[8,48,4096]{2,1,0:T(8,128)(2,1)}), bf16[8,48,4096]{2,1,0:T(8,128)(2,1)}, u32[]{:S(2)}, u32[]{:S(2)}) async-start(bf16[8,48,4096]{2,1,0:T(8,128)(2,1)} %bitcast.154), calls=%async_computation | async-start | bytes 6291456 | tf_op jit(solution)/shard_map/all_to_all | solution.py:123
  15.9 1.4 multiply_convert_fusion.1
  17.3 3.4 %collective-permute-start = (bf16[30,512]{1,0:T(8,128)(2,1)S(1)}, bf16[30,512]{1,0:T(8,128)(2,1)S(1)}, u32[]{:S(2)}, u32[]{:S(2)}) collective-permute-start(bf16[30,512]{1,0:T(8,128)(2,1)S(1)} %slice.288), channel_id=1, source_target_pairs={{0,4},{4,8},{8,12},{12,16},{16,20},{20,24},{24,28},{1,5},{5,9},{9,... | collective-permute-start | bytes 92168 | tf_op jit(solution)/shard_map/ppermute | solution.py:13
  20.7 3.2 %fusion = f32[512]{0:T(512)S(1)} fusion(bf16[512,4096]{1,0:T(8,128)(2,1)} %param.24), kind=kLoop, calls=%fused_computation.2 | loop fusion | flops 6290944 | bytes 4196352 | tf_op jit(solution)/shard_map/reduce_sum | solution.py:67
  24.1 3.0 %fusion.19 = f32[512,256]{1,0:T(8,128)S(1)} fusion(bf16[4096,256]{1,0:T(8,128)(2,1)} %param.31, bf16[512,4096]{1,0:T(8,128)(2,1)S(1)} %copy-done.2, f32[4096]{0:T(1024)S(1)} %copy-done.16, f32[512]{0:T(512)S(1)} %add_rsqrt_fusion), kind=kOutput, calls=%fused_computation.38 | convolution fusion | flops 1082130432 | bytes 6834176 | tf_op jit(solution)/shard_map/dot_general | solution.py:74
  27.2 1.3 fusion.21
  28.7 2.1 convolution_convert_fusion.1
  30.8 2.1 convolution_convert_fusion.2
  32.9 1.5 fusion.85
  34.9 49.5 %collective-permute-done = bf16[30,512]{1,0:T(8,128)(2,1)S(1)} collective-permute-done((bf16[30,512]{1,0:T(8,128)(2,1)S(1)}, bf16[30,512]{1,0:T(8,128)(2,1)S(1)}, u32[]{:S(2)}, u32[]{:S(2)}) %collective-permute-start) | collective-permute-done | bytes 30752 | tf_op jit(solution)/shard_map/ppermute | solution.py:13
  84.4 1.5 collective-permute-start.3
  86.1 5.7 %multiply_reduce_fusion = (f32[512]{0:T(512)S(1)}, f32[512]{0:T(512)}, f32[512,512]{1,0:T(8,128)S(1)}) fusion(f32[542,512]{1,0:T(8,128)S(1)} %maximum_convert_fusion, f32[512]{0:T(512)S(1)} %bitcast.179, f32[512]{0:T(512)S(1)} %bitcast.180, f32[512]{0:T(512)S(1)} %bitcast.182, f32[512]{0:T(512)S(1)} %bitcast.183, f32[512]{0:T(512)S(1)} %bitcast.184, ...), kind=kLoop, calls=%fused_computation.111 | loop fusion | flops 17038336 | bytes 33624064 | tf_op jit(solution)/shard_map/reduce_sum | solution.py:163
  91.8 3.5 %fusion.79 = f32[384,256]{1,0:T(8,128)S(1)} fusion(bf16[384,4096]{1,0:T(8,128)(2,1)} %bitcast.35, bf16[1,4096,256]{2,1,0:T(8,128)(2,1)} %param.28), kind=kOutput, calls=%fused_computation.147 | convolution fusion | flops 805306368 | bytes 5636096 | tf_op jit(solution)/shard_map/dot_general | solution.py:74
  95.4 3.5 %fusion.88 = f32[384,256]{1,0:T(8,128)S(1)} fusion(bf16[384,4096]{1,0:T(8,128)(2,1)} %bitcast.35, bf16[4096,256]{1,0:T(8,128)(2,1)} %collective-permute-done.1), kind=kOutput, calls=%fused_computation.155 | convolution fusion | flops 805306368 | bytes 5636096 | tf_op jit(solution)/shard_map/dot_general | solution.py:74
  99.2 3.7 %fusion.90 = f32[384,256]{1,0:T(8,128)S(1)} fusion(bf16[384,4096]{1,0:T(8,128)(2,1)} %bitcast.35, bf16[4096,256]{1,0:T(8,128)(2,1)} %collective-permute-done.4), kind=kOutput, calls=%fused_computation.157 | convolution fusion | flops 805306368 | bytes 5636096 | tf_op jit(solution)/shard_map/dot_general | solution.py:74
  102.9 2.9 %fusion.24 = bf16[384,256]{1,0:T(8,128)(2,1)S(1)} fusion(bf16[384,4096]{1,0:T(8,128)(2,1)} %bitcast.35, f32[384,256]{1,0:T(8,128)S(1)} %fusion.79, bf16[1,4096,256]{2,1,0:T(8,128)(2,1)S(1)} %copy-done.24), kind=kOutput, calls=%fused_computation.41 | convolution fusion | flops 805896192 | bytes 5832704 | tf_op jit(solution)/shard_map/dot_general | solution.py:75
  105.8 10.0 %collective-permute-done.3 = bf16[256,2048]{1,0:T(8,128)(2,1)} collective-permute-done((bf16[256,2048]{1,0:T(8,128)(2,1)}, bf16[256,2048]{1,0:T(8,128)(2,1)}, u32[]{:S(2)}, u32[]{:S(2)}) %collective-permute-start.3) | collective-permute-done | bytes 1048608 | tf_op jit(solution)/shard_map/ppermute | solution.py:18
  116.4 3.5 %fusion.92 = f32[384,256]{1,0:T(8,128)S(1)} fusion(bf16[384,4096]{1,0:T(8,128)(2,1)} %bitcast.35, bf16[4096,256]{1,0:T(8,128)(2,1)} %collective-permute-done.7), kind=kOutput, calls=%fused_computation.159 | convolution fusion | flops 805306368 | bytes 5636096 | tf_op jit(solution)/shard_map/dot_general | solution.py:74
  119.9 3.7 %multiply_convert_fusion.4 = bf16[384,256]{1,0:T(8,128)(2,1)S(1)} fusion(f32[384,256]{1,0:T(8,128)S(1)} %fusion.88, bf16[384,4096]{1,0:T(8,128)(2,1)} %bitcast.35, bf16[4096,256]{1,0:T(8,128)(2,1)} %collective-permute-done.2), kind=kOutput, calls=%fused_computation.117 | convolution fusion | flops 805896192 | bytes 5832704 | tf_op jit(solution)/shard_map/dot_general | solution.py:75
  124.2 3.5 %multiply_convert_fusion.3 = bf16[384,256]{1,0:T(8,128)(2,1)S(1)} fusion(f32[384,256]{1,0:T(8,128)S(1)} %fusion.90, bf16[384,4096]{1,0:T(8,128)(2,1)} %bitcast.35, bf16[4096,256]{1,0:T(8,128)(2,1)} %collective-permute-done.5), kind=kOutput, calls=%fused_computation.116 | convolution fusion | flops 805896192 | bytes 5832704 | tf_op jit(solution)/shard_map/dot_general | solution.py:75
  127.8 1.8 fusion.89
  130.2 2.9 %multiply_convert_fusion.2 = bf16[384,256]{1,0:T(8,128)(2,1)S(1)} fusion(f32[384,256]{1,0:T(8,128)S(1)} %fusion.92, bf16[384,4096]{1,0:T(8,128)(2,1)} %bitcast.35, bf16[4096,256]{1,0:T(8,128)(2,1)S(1)} %collective-permute-done.8), kind=kOutput, calls=%fused_computation.115 | convolution fusion | flops 805896192 | bytes 5832704 | tf_op jit(solution)/shard_map/dot_general | solution.py:75
  133.1 1.9 add_convert_fusion.1
  134.9 6.4 %all-to-all-start.1 = ((bf16[8,48,2048]{2,1,0:T(8,128)(2,1)}), bf16[8,48,2048]{2,1,0:T(8,128)(2,1)S(1)}, u32[]{:S(2)}, u32[]{:S(2)}) async-start(bf16[8,48,2048]{2,1,0:T(8,128)(2,1)} %bitcast.157), calls=%async_computation.1 | async-start | bytes 3145728 | tf_op jit(solution)/shard_map/all_to_all | solution.py:154
  141.3 1.5 collective-permute-start.14
  142.8 26.3 %all-reduce = (f32[512]{0:T(512)S(1)}, f32[512]{0:T(512)S(1)}) all-reduce(f32[512]{0:T(512)S(1)} %get-tuple-element.6, f32[512]{0:T(512)S(1)} %copy-done.17), channel_id=1, replica_groups=mesh['ep'=8,'tp'=4] {'tp'}, use_global_device_ids=true, to_apply=%region_5.6 | all-reduce | flops 1024 | bytes 8192 | tf_op jit(solution)/shard_map/psum | solution.py:165
  169.1 1.1 multiply_convert_fusion
  170.3 5.0 %convolution_convert_fusion.3 = bf16[256,4096]{1,0:T(8,128)(2,1)} fusion(bf16[256,512]{1,0:T(8,128)(2,1)S(1)} %bitcast.167, bf16[512,4096]{1,0:T(8,128)(2,1)} %param.23), kind=kOutput, calls=%fused_computation.8 | convolution fusion | flops 1074790400 | bytes 6553600 | tf_op jit(solution)/shard_map/dot_general | solution.py:47
  175.3 1.6 fusion.26
  176.9 0.6 collective-permute-start.13
  179.1 2.6 %convolution_convert_fusion.4 = bf16[256,4096]{1,0:T(8,128)(2,1)} fusion(bf16[256,512]{1,0:T(8,128)(2,1)S(1)} %bitcast.166, bf16[512,4096]{1,0:T(8,128)(2,1)S(1)} %copy-done.22), kind=kOutput, calls=%fused_computation.9 | convolution fusion | flops 1074790400 | bytes 6553600 | tf_op jit(solution)/shard_map/dot_general | solution.py:49
  181.7 1.8 fusion.94
  184.5 1.9 add_convert_fusion
  186.3 6.0 %all-to-all-start.2 = ((bf16[8,48,2048]{2,1,0:T(8,128)(2,1)}), bf16[8,48,2048]{2,1,0:T(8,128)(2,1)}, u32[]{:S(2)}, u32[]{:S(2)}) async-start(bf16[8,48,2048]{2,1,0:T(8,128)(2,1)} %bitcast.158), calls=%async_computation.2 | async-start | bytes 3145728 | tf_op jit(solution)/shard_map/all_to_all | solution.py:154
  192.3 1.9 fusion.25
  194.3 1.2 collective-permute-start.11
  195.4 7.7 %collective-permute-done.13 = bf16[1,128,4096]{2,1,0:T(8,128)(2,1)} collective-permute-done((bf16[1,128,4096]{2,1,0:T(8,128)(2,1)S(1)}, bf16[1,128,4096]{2,1,0:T(8,128)(2,1)}, u32[]{:S(2)}, u32[]{:S(2)}) %collective-permute-start.13) | collective-permute-done | bytes 1048608 | tf_op jit(solution)/shard_map/ppermute | solution.py:18
  203.1 2.0 fusion.16
  205.8 1.3 fusion.12
  207.1 17.8 %collective-permute-done.11 = bf16[1,128,4096]{2,1,0:T(8,128)(2,1)S(1)} collective-permute-done((bf16[1,128,4096]{2,1,0:T(8,128)(2,1)S(1)}, bf16[1,128,4096]{2,1,0:T(8,128)(2,1)S(1)}, u32[]{:S(2)}, u32[]{:S(2)}) %collective-permute-start.11) | collective-permute-done | bytes 1048608 | tf_op jit(solution)/shard_map/ppermute | solution.py:18
  224.9 2.7 %fusion.17 = bf16[128,4096]{1,0:T(8,128)(2,1)} fusion(bf16[1,128,4096]{2,1,0:T(8,128)(2,1)S(1)} %collective-permute-done.11, bf16[1,2,128,4096]{3,2,1,0:T(8,128)(2,1)} %bitcast.43, s32[]{:T(128)S(6)} %select_n.51, bf16[1,2,128,4096]{3,2,1,0:T(8,128)(2,1)S(1)} %bitcast.163), kind=kLoop, calls=%fused_computation.34 | loop fusion | flops 3145728 | bytes 4194308 | tf_op jit(solution)/shard_map/convert_element_type | solution.py:173
  227.6 2.0 fusion.10
  229.7 2.0 fusion.11
  231.7 1.1 pad_maximum_fusion
  (97 shorter events, 7.4 us)
Async XLA Ops:
  0.6 28.0 %copy-start = (bf16[256,4096]{1,0:T(8,128)(2,1)S(1)}, bf16[256,4096]{1,0:T(8,128)(2,1)}, u32[]{:S(2)}) copy-start(bf16[256,4096]{1,0:T(8,128)(2,1)} %param.33) | copy-start | bytes 6291460
  0.6 85.4 %collective-permute-start.1 = (bf16[4096,256]{1,0:T(8,128)(2,1)}, bf16[4096,256]{1,0:T(8,128)(2,1)}, u32[]{:S(2)}, u32[]{:S(2)}) collective-permute-start(bf16[4096,256]{1,0:T(8,128)(2,1)} %bitcast.201), channel_id=1, source_target_pairs={{0,2},{1,3},{2,0},{3,1},{4,6},{5,7},{6,4},{7,5},{8,10},{9,11},{10,... | collective-permute-start | bytes 6291464 | tf_op jit(solution)/shard_map/ppermute | solution.py:18
  2.2 96.7 %collective-permute-start.4 = (bf16[4096,256]{1,0:T(8,128)(2,1)}, bf16[4096,256]{1,0:T(8,128)(2,1)}, u32[]{:S(2)}, u32[]{:S(2)}) collective-permute-start(bf16[4096,256]{1,0:T(8,128)(2,1)} %bitcast.202), channel_id=1, source_target_pairs={{0,1},{1,0},{2,3},{3,2},{4,5},{5,4},{6,7},{7,6},{8,9},{9,8},{10,11... | collective-permute-start | bytes 6291464 | tf_op jit(solution)/shard_map/ppermute | solution.py:18
  2.2 113.6 %collective-permute-start.2 = (bf16[4096,256]{1,0:T(8,128)(2,1)}, bf16[4096,256]{1,0:T(8,128)(2,1)}, u32[]{:S(2)}, u32[]{:S(2)}) collective-permute-start(bf16[4096,256]{1,0:T(8,128)(2,1)} %bitcast.203), channel_id=1, source_target_pairs={{0,2},{1,3},{2,0},{3,1},{4,6},{5,7},{6,4},{7,5},{8,10},{9,11},{10,... | collective-permute-start | bytes 6291464 | tf_op jit(solution)/shard_map/ppermute | solution.py:18
  2.7 121.5 %collective-permute-start.5 = (bf16[4096,256]{1,0:T(8,128)(2,1)}, bf16[4096,256]{1,0:T(8,128)(2,1)}, u32[]{:S(2)}, u32[]{:S(2)}) collective-permute-start(bf16[4096,256]{1,0:T(8,128)(2,1)} %bitcast.204), channel_id=1, source_target_pairs={{0,1},{1,0},{2,3},{3,2},{4,5},{5,4},{6,7},{7,6},{8,9},{9,8},{10,11... | collective-permute-start | bytes 6291464 | tf_op jit(solution)/shard_map/ppermute | solution.py:18
  9.5 6.4 %copy-start.14 = (bf16[512,512]{1,0:T(8,128)(2,1)S(1)}, bf16[512,512]{1,0:T(8,128)(2,1)}, u32[]{:S(2)}) copy-start(bf16[512,512]{1,0:T(8,128)(2,1)} %param.18) | copy-start | bytes 1572868
  9.5 82.3 %all-to-all-start = ((bf16[8,48,4096]{2,1,0:T(8,128)(2,1)}), bf16[8,48,4096]{2,1,0:T(8,128)(2,1)}, u32[]{:S(2)}, u32[]{:S(2)}) async-start(bf16[8,48,4096]{2,1,0:T(8,128)(2,1)} %bitcast.154), calls=%async_computation | async-start | bytes 6291456 | tf_op jit(solution)/shard_map/all_to_all | solution.py:123
  15.9 8.0 %copy-start.16 = (f32[4096]{0:T(1024)S(1)}, f32[4096]{0:T(1024)}, u32[]{:S(2)}) copy-start(f32[4096]{0:T(1024)} %param.25) | copy-start | bytes 49156
  17.3 67.1 %collective-permute-start = (bf16[30,512]{1,0:T(8,128)(2,1)S(1)}, bf16[30,512]{1,0:T(8,128)(2,1)S(1)}, u32[]{:S(2)}, u32[]{:S(2)}) collective-permute-start(bf16[30,512]{1,0:T(8,128)(2,1)S(1)} %slice.288), channel_id=1, source_target_pairs={{0,4},{4,8},{8,12},{12,16},{16,20},{20,24},{24,28},{1,5},{5,9},{9,... | collective-permute-start | bytes 92168 | tf_op jit(solution)/shard_map/ppermute | solution.py:13
  20.7 3.5 %copy-start.2 = (bf16[512,4096]{1,0:T(8,128)(2,1)S(1)}, bf16[512,4096]{1,0:T(8,128)(2,1)}, u32[]{:S(2)}) copy-start(bf16[512,4096]{1,0:T(8,128)(2,1)} %param.24) | copy-start | bytes 12582916
  24.1 3.0 %copy-start.23 = (bf16[4096,256]{1,0:T(8,128)(2,1)S(1)}, bf16[4096,256]{1,0:T(8,128)(2,1)}, u32[]{:S(2)}) copy-start(bf16[4096,256]{1,0:T(8,128)(2,1)} %param.32) | copy-start | bytes 6291460
  27.2 1.4 copy-start.15
  30.8 2.1 copy-start.5
  32.9 1.5 copy-start.21
  32.9 53.2 %copy-start.20 = (f32[512]{0:T(512)S(1)}, f32[512]{0:T(512)}, u32[]{:S(2)}) copy-start(f32[512]{0:T(512)} %param.20) | copy-start | bytes 6148
  84.4 31.4 %collective-permute-start.3 = (bf16[256,2048]{1,0:T(8,128)(2,1)}, bf16[256,2048]{1,0:T(8,128)(2,1)}, u32[]{:S(2)}, u32[]{:S(2)}) collective-permute-start(bf16[256,2048]{1,0:T(8,128)(2,1)} %get-tuple-element.14), channel_id=1, source_target_pairs={{0,2},{1,3},{2,0},{3,1},{4,6},{5,7},{6,4},{7,5},{8,10},{9,11},{10,... | collective-permute-start | bytes 3145736 | tf_op jit(solution)/shard_map/ppermute | solution.py:18
  86.1 30.3 %collective-permute-start.7 = (bf16[4096,256]{1,0:T(8,128)(2,1)}, bf16[4096,256]{1,0:T(8,128)(2,1)}, u32[]{:S(2)}, u32[]{:S(2)}) collective-permute-start(bf16[4096,256]{1,0:T(8,128)(2,1)} %collective-permute-done.1), channel_id=1, source_target_pairs={{0,1},{1,0},{2,3},{3,2},{4,5},{5,4},{6,7},{7,6},{8,9},{9,8},{10,11... | collective-permute-start | bytes 6291464 | tf_op jit(solution)/shard_map/ppermute | solution.py:18
  98.9 4.0 %copy-start.24 = (bf16[1,4096,256]{2,1,0:T(8,128)(2,1)S(1)}, bf16[1,4096,256]{2,1,0:T(8,128)(2,1)}, u32[]{:S(2)}) copy-start(bf16[1,4096,256]{2,1,0:T(8,128)(2,1)} %param.29) | copy-start | bytes 6291460
  98.9 30.6 %collective-permute-start.6 = (bf16[256,2048]{1,0:T(8,128)(2,1)}, bf16[256,2048]{1,0:T(8,128)(2,1)S(1)}, u32[]{:S(2)}, u32[]{:S(2)}) collective-permute-start(bf16[256,2048]{1,0:T(8,128)(2,1)} %get-tuple-element.14), channel_id=1, source_target_pairs={{0,1},{1,0},{2,3},{3,2},{4,5},{5,4},{6,7},{7,6},{8,9},{9,8},{10,11... | collective-permute-start | bytes 3145736 | tf_op jit(solution)/shard_map/ppermute | solution.py:18
  105.8 17.8 %copy-start.10 = (bf16[384,256]{1,0:T(8,128)(2,1)}, bf16[384,256]{1,0:T(8,128)(2,1)S(1)}, u32[]{:S(2)}) copy-start(bf16[384,256]{1,0:T(8,128)(2,1)S(1)} %fusion.24) | copy-start | bytes 589828
  115.8 59.5 %collective-permute-start.12 = (bf16[256,4096]{1,0:T(8,128)(2,1)}, bf16[256,4096]{1,0:T(8,128)(2,1)}, u32[]{:S(2)}, u32[]{:S(2)}) collective-permute-start(bf16[256,4096]{1,0:T(8,128)(2,1)} %convolution_convert_fusion.1), channel_id=1, source_target_pairs={{0,1},{1,0},{2,3},{3,2},{4,5},{5,4},{6,7},{7,6},{8,9},{9,8},{10,11... | collective-permute-start | bytes 6291464 | tf_op jit(solution)/shard_map/ppermute | solution.py:18
  115.8 17.2 %collective-permute-start.9 = (bf16[256,2048]{1,0:T(8,128)(2,1)}, bf16[256,2048]{1,0:T(8,128)(2,1)S(1)}, u32[]{:S(2)}, u32[]{:S(2)}) collective-permute-start(bf16[256,2048]{1,0:T(8,128)(2,1)} %collective-permute-done.3), channel_id=1, source_target_pairs={{0,1},{1,0},{2,3},{3,2},{4,5},{5,4},{6,7},{7,6},{8,9},{9,8},{10,11... | collective-permute-start | bytes 3145736 | tf_op jit(solution)/shard_map/ppermute | solution.py:18
  116.3 13.8 %collective-permute-start.8 = (bf16[4096,256]{1,0:T(8,128)(2,1)}, bf16[4096,256]{1,0:T(8,128)(2,1)S(1)}, u32[]{:S(2)}, u32[]{:S(2)}) collective-permute-start(bf16[4096,256]{1,0:T(8,128)(2,1)} %collective-permute-done.2), channel_id=1, source_target_pairs={{0,1},{1,0},{2,3},{3,2},{4,5},{5,4},{6,7},{7,6},{8,9},{9,8},{10,11... | collective-permute-start | bytes 6291464 | tf_op jit(solution)/shard_map/ppermute | solution.py:18
  119.9 3.7 %copy-start.6 = (bf16[1,256,4096]{2,1,0:T(8,128)(2,1)S(1)}, bf16[1,256,4096]{2,1,0:T(8,128)(2,1)}, u32[]{:S(2)}) copy-start(bf16[1,256,4096]{2,1,0:T(8,128)(2,1)} %param.30) | copy-start | bytes 6291460
  133.0 1.9 copy-start.12
  134.9 7.9 %copy-start.17 = (f32[512]{0:T(512)S(1)}, f32[512]{0:T(512)}, u32[]{:S(2)}) copy-start(f32[512]{0:T(512)} %get-tuple-element.5) | copy-start | bytes 6148
  134.9 51.4 %all-to-all-start.1 = ((bf16[8,48,2048]{2,1,0:T(8,128)(2,1)}), bf16[8,48,2048]{2,1,0:T(8,128)(2,1)S(1)}, u32[]{:S(2)}, u32[]{:S(2)}) async-start(bf16[8,48,2048]{2,1,0:T(8,128)(2,1)} %bitcast.157), calls=%async_computation.1 | async-start | bytes 3145728 | tf_op jit(solution)/shard_map/all_to_all | solution.py:154
  141.3 36.9 %collective-permute-start.14 = (bf16[256,2048]{1,0:T(8,128)(2,1)}, bf16[256,2048]{1,0:T(8,128)(2,1)}, u32[]{:S(2)}, u32[]{:S(2)}) collective-permute-start(bf16[256,2048]{1,0:T(8,128)(2,1)} %get-tuple-element.7), channel_id=1, source_target_pairs={{0,2},{1,3},{2,0},{3,1},{4,6},{5,7},{6,4},{7,5},{8,10},{9,11},{10,... | collective-permute-start | bytes 3145736 | tf_op jit(solution)/shard_map/ppermute | solution.py:18
  170.3 5.0 %copy-start.3 = (bf16[256,4096]{1,0:T(8,128)(2,1)S(1)}, bf16[256,4096]{1,0:T(8,128)(2,1)}, u32[]{:S(2)}) copy-start(bf16[256,4096]{1,0:T(8,128)(2,1)} %convolution_convert_fusion.2) | copy-start | bytes 6291460
  175.3 2.2 copy-start.7
  175.3 2.3 %copy-start.11 = (bf16[384,256]{1,0:T(8,128)(2,1)S(1)}, bf16[384,256]{1,0:T(8,128)(2,1)}, u32[]{:S(2)}) copy-start(bf16[384,256]{1,0:T(8,128)(2,1)} %copy-done.10) | copy-start | bytes 589828
  175.3 17.0 %collective-permute-start.10 = (bf16[256,4096]{1,0:T(8,128)(2,1)}, bf16[256,4096]{1,0:T(8,128)(2,1)}, u32[]{:S(2)}, u32[]{:S(2)}) collective-permute-start(bf16[256,4096]{1,0:T(8,128)(2,1)} %convolution_convert_fusion.3), channel_id=1, source_target_pairs={{0,1},{1,0},{2,3},{3,2},{4,5},{5,4},{6,7},{7,6},{8,9},{9,8},{10,11... | collective-permute-start | bytes 6291464 | tf_op jit(solution)/shard_map/ppermute | solution.py:18
  176.9 2.2 copy-start.22
  176.9 26.2 %collective-permute-start.13 = (bf16[1,128,4096]{2,1,0:T(8,128)(2,1)S(1)}, bf16[1,128,4096]{2,1,0:T(8,128)(2,1)}, u32[]{:S(2)}, u32[]{:S(2)}) collective-permute-start(bf16[1,128,4096]{2,1,0:T(8,128)(2,1)S(1)} %fusion.26), channel_id=1, source_target_pairs={{0,2},{1,3},{2,0},{3,1},{4,6},{5,7},{6,4},{7,5},{8,10},{9,11},{10,... | collective-permute-start | bytes 3145736 | tf_op jit(solution)/shard_map/ppermute | solution.py:18
  177.5 6.0 %collective-permute-start.15 = (bf16[256,2048]{1,0:T(8,128)(2,1)S(1)}, bf16[256,2048]{1,0:T(8,128)(2,1)S(1)}, u32[]{:S(2)}, u32[]{:S(2)}) collective-permute-start(bf16[256,2048]{1,0:T(8,128)(2,1)S(1)} %copy-done.7), channel_id=1, source_target_pairs={{0,1},{1,0},{2,3},{3,2},{4,5},{5,4},{6,7},{7,6},{8,9},{9,8},{10,11... | collective-permute-start | bytes 3145736 | tf_op jit(solution)/shard_map/ppermute | solution.py:18
  178.2 5.9 %collective-permute-start.16 = (bf16[256,2048]{1,0:T(8,128)(2,1)}, bf16[256,2048]{1,0:T(8,128)(2,1)S(1)}, u32[]{:S(2)}, u32[]{:S(2)}) collective-permute-start(bf16[256,2048]{1,0:T(8,128)(2,1)} %collective-permute-done.14), channel_id=1, source_target_pairs={{0,1},{1,0},{2,3},{3,2},{4,5},{5,4},{6,7},{7,6},{8,9},{9,8},{10,11... | collective-permute-start | bytes 3145736 | tf_op jit(solution)/shard_map/ppermute | solution.py:18
  183.5 0.9 copy-start.13
  186.3 41.3 %all-to-all-start.2 = ((bf16[8,48,2048]{2,1,0:T(8,128)(2,1)}), bf16[8,48,2048]{2,1,0:T(8,128)(2,1)}, u32[]{:S(2)}, u32[]{:S(2)}) async-start(bf16[8,48,2048]{2,1,0:T(8,128)(2,1)} %bitcast.158), calls=%async_computation.2 | async-start | bytes 3145728 | tf_op jit(solution)/shard_map/all_to_all | solution.py:154
  192.3 10.8 %copy-start.4 = (bf16[256,4096]{1,0:T(8,128)(2,1)S(1)}, bf16[256,4096]{1,0:T(8,128)(2,1)}, u32[]{:S(2)}) copy-start(bf16[256,4096]{1,0:T(8,128)(2,1)} %convolution_convert_fusion.2) | copy-start | bytes 6291460
  194.3 10.9 %copy-start.19 = (f32[128]{0:T(128)S(1)}, f32[128]{0:T(128)}, u32[]{:S(2)}) copy-start(f32[128]{0:T(128)} %get-tuple-element.55) | copy-start | bytes 1540
  194.3 30.6 %collective-permute-start.11 = (bf16[1,128,4096]{2,1,0:T(8,128)(2,1)S(1)}, bf16[1,128,4096]{2,1,0:T(8,128)(2,1)S(1)}, u32[]{:S(2)}, u32[]{:S(2)}) collective-permute-start(bf16[1,128,4096]{2,1,0:T(8,128)(2,1)S(1)} %fusion.25), channel_id=1, source_target_pairs={{0,2},{1,3},{2,0},{3,1},{4,6},{5,7},{6,4},{7,5},{8,10},{9,11},{10,... | collective-permute-start | bytes 3145736 | tf_op jit(solution)/shard_map/ppermute | solution.py:18
  205.1 0.6 copy-start.18
  205.7 19.3 %copy-start.8 = (bf16[256,4096]{1,0:T(8,128)(2,1)S(1)}, bf16[256,4096]{1,0:T(8,128)(2,1)}, u32[]{:S(2)}) copy-start(bf16[256,4096]{1,0:T(8,128)(2,1)} %convolution_convert_fusion.4) | copy-start | bytes 6291460
  227.6 5.1 %copy-start.1 = (bf16[256,4096]{1,0:T(8,128)(2,1)S(1)}, bf16[256,4096]{1,0:T(8,128)(2,1)}, u32[]{:S(2)}) copy-start(bf16[256,4096]{1,0:T(8,128)(2,1)} %param.33) | copy-start | bytes 6291460
  229.7 2.0 copy-start.9
where the time goes:
time: 237 us; the launch traced here: 233 us
  waiting for transfers between devices  85.1 us (36%)
  matrix products  63 us (27%)
  starting transfers between devices  30.6 us (13%)
  blocking collectives  26.3 us (11%)
  other arithmetic  23.2 us (10%)
  local copies, waits for them, and re-layouts  3.3 us (1%)
    ppermute x1, waiting for transfers between devices, shifted(): return lax.ppermute(x, axis, pairs)  49.5 us
    ppermute x16, waiting for transfers between devices, swapped(): return lax.ppermute(x, axis, [(i, i ^ bit) for i in range(devices)])  35.6 us
    psum x1, blocking collectives, per_device(): row_sum, squares = lax.psum((row_sum, squares), 'tp')  26.3 us
    dot_general x5, matrix products, gated_hidden(): jnp.dot(rows_in, weight_gate, preferred_element_type=jnp.float32)  17.3 us
    dot_general x5, matrix products, gated_hidden(): jnp.dot(rows_in, weight_up, preferred_element_type=jnp.float32)  14.3 us
    all_to_all x2, starting transfers between devices, per_device(): lax.all_to_all(product.reshape(ep_count, capacity, chunk), 'ep', split_ax...  12.4 us
    dot_general x8, matrix products, per_device(): jnp.dot(h, piece, preferred_element_type=jnp.float32)  9.64 us
    ppermute x16, starting transfers between devices, swapped(): return lax.ppermute(x, axis, [(i, i ^ bit) for i in range(devices)])  8.56 us
  transfers between devices with their start and end apart: 20, of which 4 were waited for; matrix products, arithmetic and copies ran while one was open for 36% of the time, Pallas kernels for 0%

commit v1 on v0

v1 whole, which is shorter than its diff:
```python
import jax
import jax.numpy as jnp
from jax import lax
from jax.experimental import pallas as pl
from jax.experimental.pallas import tpu as pltpu
from jax.sharding import PartitionSpec as P


MESH = pl.DeviceIdType.MESH

EPSILON = 1e-06
COLUMN_CHUNKS = 4
TILE = 256
DEPTH = 1024
NEAR, FAR = 1, 2


def shifted(x, axis, by):
    devices = lax.axis_size(axis)
    pairs = [(i, i + by) for i in range(devices) if 0 <= i + by < devices]
    return lax.ppermute(x, axis, pairs)


def swapped(x, axis, bit):
    devices = lax.axis_size(axis)
    return lax.ppermute(x, axis, [(i, i ^ bit) for i in range(devices)])


def half_scattered(lhs, weight):
    count = lax.axis_size("tp")
    me = lax.axis_index("tp")
    rows, width = lhs.shape[0] // count, weight.shape[1]
    core, low = me % 2, me // 2
    blocks = lhs.reshape(count // 2, 2, rows, lhs.shape[1])
    sent = lax.dynamic_index_in_dim(blocks, 1 - core, 1, keepdims=False).reshape(-1, lhs.shape[1])
    kept = lax.dynamic_index_in_dim(blocks, core, 1, keepdims=False).reshape(-1, lhs.shape[1])
    sent = jnp.dot(sent, weight, preferred_element_type=jnp.float32).astype(jnp.bfloat16)
    arrived = swapped(sent, "tp", NEAR)
    kept = jnp.dot(kept, weight, preferred_element_type=jnp.float32).astype(jnp.bfloat16)
    halves = [part.reshape(count // 2, rows, width) for part in (kept, arrived)]
    give = sum(
        lax.dynamic_index_in_dim(h, 1 - low, 0, keepdims=False).astype(jnp.float32) for h in halves
    ).astype(jnp.bfloat16)
    keep = sum(
        lax.dynamic_index_in_dim(h, low, 0, keepdims=False).astype(jnp.float32) for h in halves
    )
    return give, keep


def expert_kernel(
    rows_ref,
    g0,
    g1,
    g2,
    g3,
    u0,
    u1,
    u2,
    down_ref,
    choice_ref,
    share_ref,
    give_s,
    give_m,
    keep_s,
    keep_m,
    mixer_ref,
    out_ref,
    wbuf,
    acc,
    hid,
    downs,
    prod,
    ret,
    arr,
    load_sem,
    relay_sem,
    down_send,
    down_recv,
    near_send,
    near_recv,
    rs_send,
    rs_recv,
    ret_send,
    ret_recv,
):
    me, t = lax.axis_index("ep"), lax.axis_index("tp")
    count = lax.axis_size("ep")
    chunks, _, cap, chunk = prod.shape
    near = {"tp": t + 1 - 2 * lax.rem(t, 2)}
    far = {"tp": lax.rem(t + 2, 4)}

    def remote(src, dst, send, recv, to):
        return pltpu.make_async_remote_copy(
            src_ref=src, dst_ref=dst, send_sem=send, recv_sem=recv, device_id=to, device_id_type=MESH
        )

    def cols(c):
        return pl.ds(c * chunk, chunk)

    barrier = pltpu.get_barrier_semaphore()
    pl.semaphore_signal(barrier, inc=1, device_id=near, device_id_type=MESH)
    pl.semaphore_signal(barrier, inc=1, device_id=far, device_id_type=MESH)

    @pl.loop(1, count)
    def _(j):
        pl.semaphore_signal(
            barrier, inc=1, device_id={"ep": lax.rem(me + j, count)}, device_id_type=MESH
        )

    loads = [
        pltpu.make_async_copy(src, wbuf.at[slot], load_sem.at[slot])
        for src, slot in ((g0, 0), (u0, 4), (g2, 2), (u2, 6), (g1, 1), (u1, 5), (g3, 3))
    ]
    for load in loads:
        load.start()
    pl.semaphore_wait(barrier, count + 1)

    to_far = [
        remote(
            down_ref.at[:, cols(c)], downs.at[0, :, cols(c)], down_send.at[c], down_recv.at[c], far
        )
        for c in range(chunks)
    ]
    relay = remote(u1, wbuf.at[7], relay_sem.at[0], relay_sem.at[1], near)
    to_near = [
        remote(
            down_ref.at[:, cols(c)],
            downs.at[1, :, cols(c)],
            near_send.at[0, c],
            near_recv.at[0, c],
            near,
        )
        for c in range(chunks)
    ]
    on_near = [
        remote(
            downs.at[0, :, cols(c)],
            downs.at[2, :, cols(c)],
            near_send.at[1, c],
            near_recv.at[1, c],
            near,
        )
        for c in range(chunks)
    ]
    crossings = [
        remote(give, arr.at[i], rs_send.at[i], rs_recv.at[i], far)
        for i, give in enumerate((give_s, give_m))
    ]
    for copy in to_far:
        copy.start()
    relay.start()
    for copy in to_near:
        copy.start()
    for copy in crossings:
        copy.start()

    def product(slot):
        acc[...] = jnp.zeros_like(acc)

        @pl.loop(0, rows_ref.shape[1] // DEPTH)
        def _(k):
            part = pl.ds(pl.multiple_of(k * DEPTH, DEPTH), DEPTH)
            acc[...] += jnp.dot(
                rows_ref[:, part], wbuf[slot, part, :], preferred_element_type=jnp.float32
            )

        return acc[...]

    for turn, slot in enumerate((0, 2, 1, 3)):
        if turn < 3:
            loads[2 * turn].wait()
            loads[2 * turn + 1].wait()
        else:
            loads[6].wait()
            relay.wait()
        gate = product(slot)
        gate = gate * jax.nn.sigmoid(gate)
        hid[slot] = (gate * product(slot + 4)).astype(jnp.bfloat16)

    def back(c, j):
        to = lax.rem(me + j, count)
        return remote(
            prod.at[c, to], ret.at[c, me], ret_send.at[c, to], ret_recv.at[c, me], {"ep": to}
        )

    for c in range(chunks):
        to_far[c].wait()
        on_near[c].start()
        to_near[c].wait()

        def partly(at):
            total = jnp.dot(hid[0], down_ref[:, at], preferred_element_type=jnp.float32)
            for piece, slot in ((0, 1), (1, 2)):
                total += jnp.dot(hid[slot], downs[piece, :, at], preferred_element_type=jnp.float32)
            return total

        on_near[c].wait()

        @pl.loop(0, chunk // TILE)
        def _(i):
            at = pl.ds(pl.multiple_of(c * chunk + i * TILE, TILE), TILE)
            total = partly(at)
            total += jnp.dot(hid[3], downs[2, :, at], preferred_element_type=jnp.float32)
            prod[c, :, :, pl.ds(pl.multiple_of(i * TILE, TILE), TILE)] = total.astype(
                jnp.bfloat16
            ).reshape(count, cap, TILE)

        @pl.loop(1, count)
        def _(j):
            back(c, j).start()

        ret[c, me] = prod[c, me]

    crossings[0].wait()
    for c in range(chunks):

        @pl.loop(1, count)
        def _(j):
            source = lax.rem(me + j, count)
            remote(
                prod.at[c, source],
                ret.at[c, source],
                ret_send.at[c, source],
                ret_recv.at[c, source],
                {"ep": source},
            ).wait()

        @pl.loop(0, chunk // TILE)
        def _(i):
            here = pl.ds(pl.multiple_of(i * TILE, TILE), TILE)
            at = pl.ds(pl.multiple_of(c * chunk + i * TILE, TILE), TILE)
            total = (keep_s[:, at] + arr[0, :, at].astype(jnp.float32)).astype(jnp.bfloat16)
            total = total.astype(jnp.float32)
            came = ret[c, :, :, here].reshape(count * cap, TILE)
            for k in range(choice_ref.shape[0]):
                picked = jnp.dot(choice_ref[k], came, preferred_element_type=jnp.float32)
                total += picked * share_ref[:, k : k + 1]
            out_ref[:, at] = total.astype(jnp.bfloat16)

    crossings[1].wait()

    @pl.loop(0, mixer_ref.shape[1] // TILE)
    def _(i):
        at = pl.ds(pl.multiple_of(i * TILE, TILE), TILE)
        mixer_ref[:, at] = (keep_m[:, at] + arr[1, :, at].astype(jnp.float32)).astype(jnp.bfloat16)


def experts_and_rest(rows_in, gates, ups, down, choice, share, give_s, give_m, keep_s, keep_m):
    count = lax.axis_size("ep")
    rows, width = give_s.shape
    slots, hidden = rows_in.shape[0], down.shape[0]
    cap, chunk = slots // count, width // COLUMN_CHUNKS
    far = pl.BlockSpec(memory_space=pl.ANY)
    vmem = pl.BlockSpec(memory_space=pltpu.VMEM)
    bf16, dma = jnp.bfloat16, pltpu.SemaphoreType.DMA
    return pl.pallas_call(
        expert_kernel,
        out_shape=[jax.ShapeDtypeStruct((rows, width), bf16)] * 2,
        in_specs=[vmem] + [far] * 7 + [vmem] * 7,
        out_specs=[vmem, vmem],
        scratch_shapes=[
            pltpu.VMEM((8, width, hidden), bf16),
            pltpu.VMEM((slots, hidden), jnp.float32),
            pltpu.VMEM((4, slots, hidden), bf16),
            pltpu.VMEM((3, hidden, width), bf16),
            pltpu.VMEM((COLUMN_CHUNKS, count, cap, chunk), bf16),
            pltpu.VMEM((COLUMN_CHUNKS, count, cap, chunk), bf16),
            pltpu.VMEM((2, rows, width), bf16),
            dma((8,)),
            dma((2,)),
            dma((COLUMN_CHUNKS,)),
            dma((COLUMN_CHUNKS,)),
            dma((2, COLUMN_CHUNKS)),
            dma((2, COLUMN_CHUNKS)),
            dma((2,)),
            dma((2,)),
            dma((COLUMN_CHUNKS, count)),
            dma((COLUMN_CHUNKS, count)),
        ],
        compiler_params=pltpu.CompilerParams(
            collective_id=0, has_side_effects=True, vmem_limit_bytes=63 * 2**20
        ),
        cost_estimate=pl.CostEstimate(
            flops=6 * slots * width * hidden * 4, bytes_accessed=2**24, transcendentals=0
        ),
    )(rows_in, *gates, *ups, down, choice, share, give_s, give_m, keep_s, keep_m)


def rms_normed(features, gain):
    features = features.astype(jnp.float32)
    return (
        features
        * lax.rsqrt(jnp.mean(features * features, axis=1, keepdims=True) + EPSILON)
        * gain
    ).astype(jnp.bfloat16)


def gated_hidden(rows_in, weight_gate, weight_up):
    return (
        jax.nn.silu(jnp.dot(rows_in, weight_gate, preferred_element_type=jnp.float32))
        * jnp.dot(rows_in, weight_up, preferred_element_type=jnp.float32)
    ).astype(jnp.bfloat16)


def layer(
    value_in,
    gate_in,
    conv_taps,
    conv_bias,
    ln_gain,
    ln_bias,
    out_proj,
    tokens_b,
    norm_gain,
    routes,
    route_weights,
    expert_gate,
    expert_up,
    expert_down,
    shared_gate,
    shared_up,
    shared_down,
):
    tp_count = lax.axis_size("tp")
    ep_count = lax.axis_size("ep")
    model_width = tokens_b.shape[1]
    rows_own, top_count = routes.shape
    capacity = 3 * rows_own * top_count // (2 * ep_count)
    capacity = -(-capacity // 16) * 16

    far_gate = swapped(expert_gate[0], "tp", FAR)
    gates = [expert_gate[0], far_gate]
    gates += [swapped(g, "tp", NEAR) for g in gates]

    own = lax.dynamic_slice_in_dim(tokens_b, lax.axis_index("tp") * rows_own, rows_own, 0)
    own_rows = rms_normed(own, norm_gain)
    by_choice = routes.T
    expert_ids = jnp.arange(ep_count, dtype=jnp.int32)
    names = by_choice[:, None, :] == expert_ids[None, :, None]
    named = jnp.any(names, axis=0)
    row_ids = jnp.arange(rows_own, dtype=jnp.int32)
    before_row = (row_ids[:, None] < row_ids[None, :]).astype(jnp.bfloat16)
    earlier = jnp.dot(
        named.astype(jnp.bfloat16), before_row, preferred_element_type=jnp.float32
    ).astype(jnp.int32)
    slots = jnp.arange(capacity, dtype=jnp.int32)
    placed = earlier[:, None, :] == slots[None, :, None]
    pick = (placed & named[:, None, :]).astype(jnp.bfloat16).reshape(-1, rows_own)
    outbox = jnp.dot(pick, own_rows, preferred_element_type=jnp.float32).astype(jnp.bfloat16)
    arrived = lax.all_to_all(
        outbox.reshape(ep_count, capacity, model_width), "ep", split_axis=0, concat_axis=0, tiled=True
    ).reshape(ep_count * capacity, model_width)

    gated = (value_in.astype(jnp.float32) * jax.nn.sigmoid(gate_in.astype(jnp.float32))).astype(
        jnp.bfloat16
    )
    rim_rows = conv_taps.shape[0] - 1
    length = gated.shape[0]
    before = shifted(gated[length - rim_rows :], "ep", 1)
    padded = jnp.concatenate([before, gated], axis=0).astype(jnp.float32)
    filtered = jnp.zeros(gated.shape, jnp.float32) + conv_bias[None, :]
    for tap_index in range(rim_rows + 1):
        filtered = filtered + conv_taps[tap_index][None, :] * padded[tap_index : tap_index + length]
    sums = jnp.stack([jnp.sum(filtered, axis=1), jnp.sum(filtered * filtered, axis=1)])
    near = sums + swapped(sums, "tp", 1)
    far = swapped(near, "tp", 2)
    wide, near_kept = lax.optimization_barrier((expert_up[0], near))
    far_up = swapped(wide, "tp", FAR)
    ups = [wide, far_up, swapped(wide, "tp", NEAR)]
    row_sum, squares = near_kept + far
    normed_b = rms_normed(tokens_b, norm_gain)
    hidden_shared = gated_hidden(normed_b, shared_gate, shared_up)
    give_s, keep_s = half_scattered(hidden_shared, shared_down)
    channel_count = filtered.shape[1] * tp_count
    average = row_sum / channel_count
    variance = squares / channel_count - average * average
    scale = lax.rsqrt(variance + EPSILON)
    normed_a = (filtered - average[:, None]) * scale[:, None] * ln_gain + ln_bias
    activated = jax.nn.silu(normed_a).astype(jnp.bfloat16)
    give_m, keep_m = half_scattered(activated, out_proj)

    choice = jnp.stack(
        [
            (placed & names[k][:, None, :]).astype(jnp.bfloat16).reshape(-1, rows_own).T
            for k in range(top_count)
        ]
    )
    mixer_rows, outs = experts_and_rest(
        arrived,
        gates,
        ups,
        expert_down[0],
        choice,
        route_weights,
        give_s,
        give_m,
        keep_s,
        keep_m,
    )
    return (mixer_rows, outs)


def solution(mesh):
    return jax.shard_map(
        layer,
        mesh=mesh,
        in_specs=(
            P("ep", "tp"),
            P("ep", "tp"),
            P(None, "tp"),
            P("tp"),
            P("tp"),
            P("tp"),
            P("tp", None),
            P("ep", None),
            P(),
            P(("ep", "tp"), None),
            P(("ep", "tp"), None),
            P("ep", None, "tp"),
            P("ep", None, "tp"),
            P("ep", "tp", None),
            P(None, "tp"),
            P(None, "tp"),
            P("tp", None),
        ),
        out_specs=(P(("ep", "tp"), None), P(("ep", "tp"), None)),
        check_vma=False,
    )
```

time: 237 us -> 237 us (level)
  Pallas kernels: 0 us -> 101 us
  matrix products: 63 us -> 15.7 us
  blocking collectives: 26.3 us -> 0 us
  starting transfers between devices: 30.6 us -> 13.5 us
  waiting for transfers between devices: 85.1 us -> 74.2 us
  local copies, waits for them, and re-layouts: 3.3 us -> 7.13 us
  other arithmetic: 23.2 us -> 20.5 us
    pallas_call x0 -> x1, Pallas kernels: none -> 101 us  [experts_and_rest(): pl.pallas_call(expert_kernel, out_shape=[jax.ShapeDtypeStruct((rows, widt...]
    ppermute x1, waiting for transfers between devices: 49.5 us -> 0.01 us  [shifted(): return lax.ppermute(x, axis, pairs)]
    ppermute x16 -> x9, waiting for transfers between devices: 35.6 us -> 74.2 us  [swapped(): return lax.ppermute(x, axis, [(i, i ^ bit) for i in range(devices)])]
    psum x1 -> x0, blocking collectives: 26.3 us -> none  [per_device(): row_sum, squares = lax.psum((row_sum, squares), 'tp')]
    dot_general x18 -> x6, matrix products: 31.4 us -> 10.8 us  [the longest x2 4.68 us: half_scattered(): jnp.dot(sent, weight, preferred_element_type=jnp.float32)]
    dot_general x5 -> x1, matrix products: 17.3 us -> 3.64 us  [gated_hidden(): jnp.dot(rows_in, weight_gate, preferred_element_type=jnp.float32)]
    all_to_all x3 -> x1, starting transfers between devices: 18.7 us -> 5.4 us  [layer(): lax.all_to_all(outbox.reshape(ep_count, capacity, model_width), 'ep', spl...]
    dot_general x5 -> x1, matrix products: 14.3 us -> 1.33 us  [gated_hidden(): jnp.dot(rows_in, weight_up, preferred_element_type=jnp.float32)]
  transfers between devices with their start and end apart: 20 -> 11, of which waited for: 4 -> 3; matrix products, arithmetic and copies ran while one was open for 36% -> 16% of each run, Pallas kernels for 0% -> 0%
where the time goes in v1:
time: 237 us; the launch traced here: 233 us
  Pallas kernels  101 us (43%)
  waiting for transfers between devices  74.2 us (31%)
  other arithmetic  20.5 us (9%)
  matrix products  15.7 us (7%)
  starting transfers between devices  13.5 us (6%)
  local copies, waits for them, and re-layouts  7.13 us (3%)
    pallas_call x1, Pallas kernels, experts_and_rest(): pl.pallas_call(expert_kernel, out_shape=[jax.ShapeDtypeStruct((rows, widt...  101 us
    ppermute x9, waiting for transfers between devices, swapped(): return lax.ppermute(x, axis, [(i, i ^ bit) for i in range(devices)])  74.2 us
    add x2, other arithmetic, half_scattered(): sum((lax.dynamic_index_in_dim(h, low, 0, keepdims=False).astype(jnp.float...  7.77 us
    unnamed x31, local copies, waits for them, and re-layouts  6.27 us
    all_to_all x1, starting transfers between devices, layer(): lax.all_to_all(outbox.reshape(ep_count, capacity, model_width), 'ep', spl...  5.4 us
    reduce_sum x1, other arithmetic, layer(): jnp.sum(filtered, axis=1)  5.04 us
    reduce_sum x2, other arithmetic, rms_normed(): jnp.mean(features * features, axis=1, keepdims=True) + EPSILON  4.75 us
  transfers between devices with their start and end apart: 11, of which 3 were waited for; matrix products, arithmetic and copies ran while one was open for 16% of the time, Pallas kernels for 0%

profile of v1, /device:TPU:12, one launch (start us, length us, event | category | flops | bytes accessed | tf_op | source)
XLA Modules:
  0.0 232.7 jit_solution(8359156435828222180)
XLA Ops:
  0.6 1.5 multiply_convert_fusion.1
  2.1 3.4 %collective-permute-start.3 = (bf16[30,512]{1,0:T(8,128)(2,1)S(1)}, bf16[30,512]{1,0:T(8,128)(2,1)S(1)}, u32[]{:S(2)}, u32[]{:S(2)}) collective-permute-start(bf16[30,512]{1,0:T(8,128)(2,1)S(1)} %slice.260), channel_id=1, source_target_pairs={{0,4},{4,8},{8,12},{12,16},{16,20},{20,24},{24,28},{1,5},{5,9},{9,... | collective-permute-start | bytes 92168 | tf_op jit(solution)/shard_map/ppermute | solution.py:21
  5.6 0.0 copy-start.4
  5.6 0.0 copy-start.12
  5.6 3.2 %fusion = f32[512]{0:T(512)S(1)} fusion(bf16[512,4096]{1,0:T(8,128)(2,1)} %param.24), kind=kLoop, calls=%fused_computation.2 | loop fusion | flops 6290944 | bytes 4196352 | tf_op jit(solution)/shard_map/reduce_sum | solution.py:293
  8.9 0.0 copy-start
  8.9 0.0 copy-start.13
  8.9 3.6 %fusion.7 = f32[512,256]{1,0:T(8,128)S(1)} fusion(bf16[4096,256]{1,0:T(8,128)(2,1)S(1)} %copy-done.12, bf16[512,4096]{1,0:T(8,128)(2,1)} %param.24, f32[4096]{0:T(1024)S(1)} %copy-done.4, f32[512]{0:T(512)S(1)} %add_rsqrt_fusion.1), kind=kOutput, calls=%fused_computation.20 | convolution fusion | flops 1082130432 | bytes 6834176 | tf_op jit(solution)/shard_map/dot_general | solution.py:300
  12.6 0.5 copy-done.13
  13.0 1.3 fusion.9
  14.4 0.2 copy-done.1
  14.6 2.0 convolution_convert_fusion.3
  16.7 1.5 fusion.3
  18.2 0.1 convolution_convert_fusion.5
  18.4 0.1 copy.21
  18.5 0.1 copy.23
  18.7 0.1 eq.44
  18.8 0.1 copy.22
  19.0 0.1 and_bitcast_fusion.1
  19.0 4.0 %convolution_convert_fusion = bf16[384,4096]{1,0:T(8,128)(2,1)} fusion(f32[4096]{0:T(1024)S(1)} %copy-done.4, f32[128]{0:T(128)S(1)} %add_rsqrt_fusion.2, bf16[512,4096]{1,0:T(8,128)(2,1)} %param.24, s32[]{:T(128)S(6)} %select_n.40, pred[384,128]{0,1:T(32,128)(4,1)S(1)} %get-tuple-element.9, pred[384,128]{0,1:T(32,128)(4,1)S(1)} %copy.22), kind=kOutput, calls=%fused_computation.5 | convolution fusion | flops 406372352 | bytes 4309508 | tf_op jit(solution)/shard_map/dot_general | solution.py:349
  23.0 5.4 %all-to-all-start = ((bf16[8,48,4096]{2,1,0:T(8,128)(2,1)}), bf16[8,48,4096]{2,1,0:T(8,128)(2,1)}, u32[]{:S(2)}, u32[]{:S(2)}) async-start(bf16[8,48,4096]{2,1,0:T(8,128)(2,1)} %bitcast.3), calls=%async_computation | async-start | bytes 6291456 | tf_op jit(solution)/shard_map/all_to_all | solution.py:350
  28.4 1.5 collective-permute-start
  30.0 0.2 maximum_convert_fusion
  30.1 0.0 copy-start.6
  30.2 0.0 copy-start.7
  30.2 0.0 copy-start.10
  30.2 5.0 %fusion.53 = (f32[512]{0:T(512)S(1)}, f32[512]{0:T(512)S(1)}, f32[512,512]{1,0:T(8,128)S(1)}) fusion(f32[542,512]{1,0:T(8,128)S(1)} %maximum_convert_fusion, f32[512]{0:T(512)S(1)} %bitcast.133, f32[512]{0:T(512)S(1)} %bitcast.134, f32[512]{0:T(512)S(1)} %bitcast.105, f32[512]{0:T(512)S(1)} %bitcast.106, f32[512]{0:T(512)S(1)} %bitcast.107, ...), kind=kLoop, calls=%fused_computation.116 | loop fusion | flops 17038336 | bytes 33624064 | tf_op jit(solution)/shard_map/reduce_sum | solution.py:364
  35.2 0.1 collective-permute-start.4
  35.3 1.2 collective-permute-done.4
  36.5 0.6 collective-permute-start.8
  37.1 39.2 %collective-permute-done.8 = f32[2,512]{1,0:T(2,128)S(1)} collective-permute-done((f32[2,512]{1,0:T(2,128)S(1)}, f32[2,512]{1,0:T(2,128)S(1)}, u32[]{:S(2)}, u32[]{:S(2)}) %collective-permute-start.8) | collective-permute-done | bytes 4128 | tf_op jit(solution)/shard_map/ppermute | solution.py:26
  76.3 0.4 multiply_convert_fusion
  76.8 2.6 %convolution_convert_fusion.1 = bf16[256,4096]{1,0:T(8,128)(2,1)} fusion(bf16[256,512]{1,0:T(8,128)(2,1)S(1)} %bitcast.93, bf16[512,4096]{1,0:T(8,128)(2,1)S(1)} %copy-done.10), kind=kOutput, calls=%fused_computation.6 | convolution fusion | flops 1074790400 | bytes 6553600 | tf_op jit(solution)/shard_map/dot_general | solution.py:37
  79.4 0.5 collective-permute-start.1
  80.0 0.2 copy.24
  80.1 0.7 copy.25.share_ref
  80.9 1.5 collective-permute-start.5
  82.4 0.5 collective-permute-start.2
  82.9 0.7 add_convert_fusion.2.choice_ref
  83.6 0.7 convolution_convert_fusion.4
  84.3 1.5 copy-done.11
  85.8 1.3 convolution_convert_fusion.2
  87.1 3.9 %add_bitcast_fusion.1 = (f32[128,4096]{1,0:T(8,128)}, bf16[128,4096]{1,0:T(8,128)(2,1)}) fusion(bf16[2,128,4096]{2,1,0:T(8,128)(2,1)} %bitcast.53, s32[]{:T(128)S(6)} %select_n.46, bf16[2,128,4096]{2,1,0:T(8,128)(2,1)S(1)} %bitcast.86, s32[]{:T(128)S(6)} %select_n.44), kind=kLoop, calls=%fused_computation.16 | loop fusion | flops 3670016 | bytes 7340040 | tf_op jit(solution)/shard_map/add | solution.py:44
  90.9 3.9 %add_bitcast_fusion = (f32[128,4096]{1,0:T(8,128)}, bf16[128,4096]{1,0:T(8,128)(2,1)}) fusion(bf16[2,128,4096]{2,1,0:T(8,128)(2,1)} %bitcast.61, s32[]{:T(128)S(6)} %select_n.46, bf16[2,128,4096]{2,1,0:T(8,128)(2,1)S(1)} %bitcast.88, s32[]{:T(128)S(6)} %select_n.44), kind=kLoop, calls=%fused_computation.15 | loop fusion | flops 3670016 | bytes 7340040 | tf_op jit(solution)/shard_map/add | solution.py:44
  94.8 33.9 %collective-permute-done.5.u1 = bf16[4096,256]{1,0:T(8,128)(2,1)} collective-permute-done((bf16[4096,256]{1,0:T(8,128)(2,1)}, bf16[4096,256]{1,0:T(8,128)(2,1)}, u32[]{:S(2)}, u32[]{:S(2)}) %collective-permute-start.5) | collective-permute-done | bytes 2097184 | tf_op jit(solution)/shard_map/ppermute | solution.py:26
  128.7 100.6 %shard_map.176 = (bf16[128,4096]{1,0:T(8,128)(2,1)}, bf16[128,4096]{1,0:T(8,128)(2,1)}) custom-call(bf16[384,4096]{1,0:T(8,128)(2,1)} %bitcast.4.rows_ref, bf16[4096,256]{1,0:T(8,128)(2,1)} %bitcast.5.g0, bf16[4096,256]{1,0:T(8,128)(2,1)} %collective-permute-done.g1, bf16[4096,256]{1,0:T(8,128)(2,1)} %collective-permute-done.1.g2, ...), custom_call_target="tpu_custom_call" | custom-call | flops 9663676416 | bytes 16777216 | tf_op jit(solution)/shard_map/pallas_call | solution.py:256
  229.4 2.4 %copy.33 = bf16[128,4096]{1,0:T(8,128)(2,1)} copy(bf16[128,4096]{1,0:T(8,128)(2,1)} %get-tuple-element.58) | data formatting | bytes 2097152
  231.7 1.0 copy.34
  (49 shorter events, 0.4 us)
Async XLA Ops:
  2.1 27.8 %collective-permute-start.3 = (bf16[30,512]{1,0:T(8,128)(2,1)S(1)}, bf16[30,512]{1,0:T(8,128)(2,1)S(1)}, u32[]{:S(2)}, u32[]{:S(2)}) collective-permute-start(bf16[30,512]{1,0:T(8,128)(2,1)S(1)} %slice.260), channel_id=1, source_target_pairs={{0,4},{4,8},{8,12},{12,16},{16,20},{20,24},{24,28},{1,5},{5,9},{9,... | collective-permute-start | bytes 92168 | tf_op jit(solution)/shard_map/ppermute | solution.py:21
  5.6 3.3 %copy-start.4 = (f32[4096]{0:T(1024)S(1)}, f32[4096]{0:T(1024)}, u32[]{:S(2)}) copy-start(f32[4096]{0:T(1024)} %param.25) | copy-start | bytes 49156
  5.6 3.3 %copy-start.12 = (bf16[4096,256]{1,0:T(8,128)(2,1)S(1)}, bf16[4096,256]{1,0:T(8,128)(2,1)}, u32[]{:S(2)}) copy-start(bf16[4096,256]{1,0:T(8,128)(2,1)} %param.31) | copy-start | bytes 6291460
  8.9 3.7 %copy-start = (bf16[512,4096]{1,0:T(8,128)(2,1)S(1)}, bf16[512,4096]{1,0:T(8,128)(2,1)}, u32[]{:S(2)}) copy-start(bf16[512,4096]{1,0:T(8,128)(2,1)} %param.24) | copy-start | bytes 12582916
  8.9 4.1 %copy-start.13 = (bf16[4096,256]{1,0:T(8,128)(2,1)S(1)}, bf16[4096,256]{1,0:T(8,128)(2,1)}, u32[]{:S(2)}) copy-start(bf16[4096,256]{1,0:T(8,128)(2,1)} %param.32) | copy-start | bytes 6291460
  13.0 1.6 copy-start.1
  14.6 3.6 %copy-start.9 = (s32[128,2]{0,1:T(2,128)S(1)}, s32[128,2]{0,1:T(2,128)}, u32[]{:S(2)}) copy-start(s32[128,2]{0,1:T(2,128)} %param.26) | copy-start | bytes 3076
  16.7 65.7 %collective-permute-start.7 = (bf16[256,4096]{1,0:T(8,128)(2,1)}, bf16[256,4096]{1,0:T(8,128)(2,1)}, u32[]{:S(2)}, u32[]{:S(2)}) collective-permute-start(bf16[256,4096]{1,0:T(8,128)(2,1)} %convolution_convert_fusion.3), channel_id=1, source_target_pairs={{0,1},{1,0},{2,3},{3,2},{4,5},{5,4},{6,7},{7,6},{8,9},{9,8},{10,11... | collective-permute-start | bytes 6291464 | tf_op jit(solution)/shard_map/ppermute | solution.py:26
  23.0 6.9 %copy-start.3 = (f32[31,512]{1,0:T(8,128)S(1)}, f32[31,512]{1,0:T(8,128)}, u32[]{:S(2)}) copy-start(f32[31,512]{1,0:T(8,128)} %param.19) | copy-start | bytes 190468
  23.0 7.1 %copy-start.5 = (f32[512]{0:T(512)S(1)}, f32[512]{0:T(512)}, u32[]{:S(2)}) copy-start(f32[512]{0:T(512)} %param.20) | copy-start | bytes 6148
  23.0 105.7 %all-to-all-start = ((bf16[8,48,4096]{2,1,0:T(8,128)(2,1)}), bf16[8,48,4096]{2,1,0:T(8,128)(2,1)}, u32[]{:S(2)}, u32[]{:S(2)}) async-start(bf16[8,48,4096]{2,1,0:T(8,128)(2,1)} %bitcast.3), calls=%async_computation | async-start | bytes 6291456 | tf_op jit(solution)/shard_map/all_to_all | solution.py:350
  28.4 54.0 %collective-permute-start = (bf16[4096,256]{1,0:T(8,128)(2,1)}, bf16[4096,256]{1,0:T(8,128)(2,1)}, u32[]{:S(2)}, u32[]{:S(2)}) collective-permute-start(bf16[4096,256]{1,0:T(8,128)(2,1)} %bitcast.5.g0), channel_id=1, source_target_pairs={{0,2},{1,3},{2,0},{3,1},{4,6},{5,7},{6,4},{7,5},{8,10},{9,11},{10,... | collective-permute-start | bytes 6291464 | tf_op jit(solution)/shard_map/ppermute | solution.py:26
  30.1 46.1 %copy-start.6 = (f32[512]{0:T(512)S(1)}, f32[512]{0:T(512)}, u32[]{:S(2)}) copy-start(f32[512]{0:T(512)} %param.22) | copy-start | bytes 6148
  30.2 46.1 %copy-start.7 = (f32[512]{0:T(512)S(1)}, f32[512]{0:T(512)}, u32[]{:S(2)}) copy-start(f32[512]{0:T(512)} %param.21) | copy-start | bytes 6148
  30.2 46.6 %copy-start.10 = (bf16[512,4096]{1,0:T(8,128)(2,1)S(1)}, bf16[512,4096]{1,0:T(8,128)(2,1)}, u32[]{:S(2)}) copy-start(bf16[512,4096]{1,0:T(8,128)(2,1)} %param.23) | copy-start | bytes 12582916
  35.2 1.2 collective-permute-start.4
  36.5 39.8 %collective-permute-start.8 = (f32[2,512]{1,0:T(2,128)S(1)}, f32[2,512]{1,0:T(2,128)S(1)}, u32[]{:S(2)}, u32[]{:S(2)}) collective-permute-start(f32[2,512]{1,0:T(2,128)S(1)} %fusion.52), channel_id=1, source_target_pairs={{0,2},{1,3},{2,0},{3,1},{4,6},{5,7},{6,4},{7,5},{8,10},{9,11},{10,... | collective-permute-start | bytes 12296 | tf_op jit(solution)/shard_map/ppermute | solution.py:26
  76.8 3.3 %copy-start.8 = (f32[128,2]{0,1:T(2,128)S(1)}, f32[128,2]{0,1:T(2,128)}, u32[]{:S(2)}) copy-start(f32[128,2]{0,1:T(2,128)} %param.27) | copy-start | bytes 3076
  79.4 11.5 %collective-permute-start.9 = (bf16[256,4096]{1,0:T(8,128)(2,1)}, bf16[256,4096]{1,0:T(8,128)(2,1)}, u32[]{:S(2)}, u32[]{:S(2)}) collective-permute-start(bf16[256,4096]{1,0:T(8,128)(2,1)} %convolution_convert_fusion.1), channel_id=1, source_target_pairs={{0,1},{1,0},{2,3},{3,2},{4,5},{5,4},{6,7},{7,6},{8,9},{9,8},{10,11... | collective-permute-start | bytes 6291464 | tf_op jit(solution)/shard_map/ppermute | solution.py:26
  79.4 15.4 %collective-permute-start.1 = (bf16[4096,256]{1,0:T(8,128)(2,1)}, bf16[4096,256]{1,0:T(8,128)(2,1)}, u32[]{:S(2)}, u32[]{:S(2)}) collective-permute-start(bf16[4096,256]{1,0:T(8,128)(2,1)} %bitcast.5.g0), channel_id=1, source_target_pairs={{0,1},{1,0},{2,3},{3,2},{4,5},{5,4},{6,7},{7,6},{8,9},{9,8},{10,11... | collective-permute-start | bytes 6291464 | tf_op jit(solution)/shard_map/ppermute | solution.py:26
  80.9 47.9 %collective-permute-start.5 = (bf16[4096,256]{1,0:T(8,128)(2,1)}, bf16[4096,256]{1,0:T(8,128)(2,1)}, u32[]{:S(2)}, u32[]{:S(2)}) collective-permute-start(bf16[4096,256]{1,0:T(8,128)(2,1)} %bitcast.137), channel_id=1, source_target_pairs={{0,2},{1,3},{2,0},{3,1},{4,6},{5,7},{6,4},{7,5},{8,10},{9,11},{10,... | collective-permute-start | bytes 6291464 | tf_op jit(solution)/shard_map/ppermute | solution.py:26
  82.4 46.4 %collective-permute-start.6 = (bf16[4096,256]{1,0:T(8,128)(2,1)}, bf16[4096,256]{1,0:T(8,128)(2,1)}, u32[]{:S(2)}, u32[]{:S(2)}) collective-permute-start(bf16[4096,256]{1,0:T(8,128)(2,1)} %bitcast.138), channel_id=1, source_target_pairs={{0,1},{1,0},{2,3},{3,2},{4,5},{5,4},{6,7},{7,6},{8,9},{9,8},{10,11... | collective-permute-start | bytes 6291464 | tf_op jit(solution)/shard_map/ppermute | solution.py:26
  82.4 46.4 %collective-permute-start.2 = (bf16[4096,256]{1,0:T(8,128)(2,1)}, bf16[4096,256]{1,0:T(8,128)(2,1)}, u32[]{:S(2)}, u32[]{:S(2)}) collective-permute-start(bf16[4096,256]{1,0:T(8,128)(2,1)} %collective-permute-done.g1), channel_id=1, source_target_pairs={{0,1},{1,0},{2,3},{3,2},{4,5},{5,4},{6,7},{7,6},{8,9},{9,8},{10,11... | collective-permute-start | bytes 6291464 | tf_op jit(solution)/shard_map/ppermute | solution.py:26
  83.6 2.2 copy-start.11
  229.4 2.4 %copy-start.2 = (bf16[128,4096]{1,0:T(8,128)(2,1)S(1)}, bf16[128,4096]{1,0:T(8,128)(2,1)}, u32[]{:S(2)}) copy-start(bf16[128,4096]{1,0:T(8,128)(2,1)} %get-tuple-element.59) | copy-start | bytes 3145732

commit v2 on v0

v2 whole, which is shorter than its diff:
```python
import jax
import jax.numpy as jnp
from jax import lax
from jax.experimental import pallas as pl
from jax.experimental.pallas import tpu as pltpu
from jax.sharding import PartitionSpec as P

MESH = pl.DeviceIdType.MESH
EPSILON = 1e-06
CHUNKS = 4
TILE = 256
STEP = 32
RIM = 32
F32, BF16 = jnp.float32, jnp.bfloat16


def dot(a, b):
    return jnp.dot(a, b, preferred_element_type=F32)


def silu(v):
    return v * jax.nn.sigmoid(v)


def aligned(i, size):
    return pl.ds(pl.multiple_of(i * size, size), size)


def kernel(
    value,
    gate,
    taps,
    bias,
    ln_gain,
    ln_bias,
    norm_gain,
    routes,
    share,
    out_proj,
    tokens,
    expert_gate,
    expert_up,
    expert_down,
    shared_gate,
    shared_up,
    shared_down,
    mixer_ref,
    out_ref,
    wbuf,
    opbuf,
    downs,
    tok,
    box,
    rows,
    ret,
    pad,
    act,
    hs,
    ns,
    kept,
    nr,
    arr,
    sacc,
    gacc,
    hid,
    stat,
    cols_st,
    choice,
    load,
    put_sem,
    tok_load,
    halo_sem,
    stat_sem,
    w_send,
    w_recv,
    down_send,
    down_recv,
    near_send,
    near_recv,
    rs_near,
    rs_far,
    go_send,
    go_recv,
    ret_send,
    ret_recv,
):
    me, t = lax.axis_index("ep"), lax.axis_index("tp")
    count = lax.axis_size("ep")
    _, _, cap, chunk = box.shape
    own = share.shape[0]
    length, width = value.shape[0], tok.shape[1]
    slots = count * cap
    core, low = lax.rem(t, 2), t // 2
    near = {"tp": t + 1 - 2 * core}
    far = {"tp": lax.rem(t + 2, 4)}
    hidden = hs.shape[1]

    def remote(src, dst, send, recv, to):
        return pltpu.make_async_remote_copy(
            src_ref=src, dst_ref=dst, send_sem=send, recv_sem=recv, device_id=to, device_id_type=MESH
        )

    def fetch(src, dst, i):
        return pltpu.make_async_copy(src, dst, load.at[i])

    def cols(c):
        return pl.ds(c * chunk, chunk)

    barrier = pltpu.get_barrier_semaphore()
    pl.semaphore_signal(barrier, inc=1, device_id=near, device_id_type=MESH)
    pl.semaphore_signal(barrier, inc=1, device_id=far, device_id_type=MESH)

    @pl.loop(1, count)
    def _(j):
        pl.semaphore_signal(
            barrier, inc=1, device_id={"ep": lax.rem(me + j, count)}, device_id_type=MESH
        )

    def tokens_load(b):
        return pltpu.make_async_copy(tokens.at[aligned(b, own)], tok.at[aligned(b, own)], tok_load.at[b])

    tokens_load(t).start()
    get_sg = fetch(shared_gate, wbuf.at[0], 0)
    get_su = fetch(shared_up, wbuf.at[4], 1)
    get_sd = fetch(shared_down, opbuf.at[pl.ds(0, hidden)], 2)
    get_sg.start()
    get_su.start()
    get_sd.start()

    @pl.loop(1, 4)
    def _(j):
        tokens_load(lax.rem(t + j, 4)).start()

    pl.semaphore_wait(barrier, count + 1)

    gate_far = remote(expert_gate, wbuf.at[1], w_send.at[0], w_recv.at[0], far)
    gate_near = remote(expert_gate, wbuf.at[2], w_send.at[1], w_recv.at[1], near)
    gate_on = remote(wbuf.at[1], wbuf.at[3], w_send.at[2], w_recv.at[2], near)
    up_far = remote(expert_up, wbuf.at[5], w_send.at[3], w_recv.at[3], far)
    up_near = remote(expert_up, wbuf.at[6], w_send.at[4], w_recv.at[4], near)
    up_on = remote(wbuf.at[5], wbuf.at[7], w_send.at[5], w_recv.at[5], near)
    down_far = [
        remote(expert_down.at[:, cols(c)], downs.at[0, :, cols(c)], down_send.at[c], down_recv.at[c], far)
        for c in range(CHUNKS)
    ]
    down_near = [
        remote(
            expert_down.at[:, cols(c)],
            downs.at[1, :, cols(c)],
            near_send.at[0, c],
            near_recv.at[0, c],
            near,
        )
        for c in range(CHUNKS)
    ]
    down_on = [
        remote(
            downs.at[0, :, cols(c)],
            downs.at[2, :, cols(c)],
            near_send.at[1, c],
            near_recv.at[1, c],
            near,
        )
        for c in range(CHUNKS)
    ]
    gate_far.start()
    gate_near.start()

    @pl.loop(0, length // STEP)
    def _(i):
        at = aligned(i, STEP)
        gated = value[at, :].astype(F32) * jax.nn.sigmoid(gate[at, :].astype(F32))
        pad[aligned(i + 1, STEP), :] = gated.astype(BF16).astype(F32)

    def halo(to):
        return remote(
            pad.at[pl.ds(length, RIM)], pad.at[pl.ds(0, RIM)], halo_sem.at[0], halo_sem.at[1], {"ep": to}
        )

    @pl.when(me < count - 1)
    def _():
        halo(lax.rem(me + 1, count)).start()

    @pl.when(me == 0)
    def _():
        pad[pl.ds(0, RIM), :] = jnp.zeros((RIM, pad.shape[1]), F32)

    def normalize(b):
        tokens_load(b).wait()

        @pl.loop(0, own // 16)
        def _(i):
            at = pl.ds(pl.multiple_of(b * own + i * 16, 16), 16)
            x = tok[at, :].astype(F32)
            scale = lax.rsqrt(jnp.mean(x * x, axis=1, keepdims=True) + EPSILON)
            tok[at, :] = (x * scale * norm_gain[...]).astype(BF16)

    normalize(t)
    lanes = lax.broadcasted_iota(jnp.int32, (own, 128), 1)
    names = [(lanes == routes[:, k : k + 1]).astype(F32) for k in range(routes.shape[1])]
    before = lax.broadcasted_iota(jnp.int32, (own, own), 1) < lax.broadcasted_iota(
        jnp.int32, (own, own), 0
    )
    earlier = dot(before.astype(F32).astype(BF16), sum(names).astype(BF16))
    places = lax.broadcasted_iota(jnp.int32, (own, slots), 1).astype(F32)
    anywhere = jnp.zeros((own, slots), F32)
    for k, name in enumerate(names):
        place = jnp.sum(earlier * name, axis=1, keepdims=True)
        place = place + routes[:, k : k + 1].astype(F32) * cap
        chosen = (places == place).astype(F32)
        anywhere = anywhere + chosen
        choice[k] = chosen.astype(BF16)
    pick = anywhere.T.astype(BF16)

    def going(c, j):
        to = lax.rem(me + j, count)
        return remote(box.at[c, to], rows.at[c, me], go_send.at[c, to], go_recv.at[c, me], {"ep": to})

    for c in range(CHUNKS):

        @pl.loop(0, chunk // TILE)
        def _(i):
            at = pl.ds(pl.multiple_of(c * chunk + i * TILE, TILE), TILE)
            sent = dot(pick, tok[aligned(t, own), at]).astype(BF16)
            box[c, :, :, aligned(i, TILE)] = sent.reshape(count, cap, TILE)

        @pl.loop(1, count)
        def _(j):
            going(c, j).start()

        rows[c, me] = box[c, me]

    @pl.when(me < count - 1)
    def _():
        halo(lax.rem(me + 1, count)).wait_send()

    @pl.when(me > 0)
    def _():
        halo(lax.rem(me + 1, count)).wait_recv()

    tap_count = taps.shape[0]
    first = RIM - (tap_count - 1)

    @pl.loop(0, length // STEP)
    def _(i):
        window = pad[pl.ds(pl.multiple_of(i * STEP, STEP), STEP + RIM), :]
        total = jnp.zeros((STEP, window.shape[1]), F32) + bias[...]
        for s in range(8):
            turned = pltpu.roll(window, STEP + RIM - s, 0) if s else window
            for q in range((RIM + 8) // 8):
                j = s + 8 * q - first
                if 0 <= j < tap_count:
                    total = total + taps[j : j + 1, :] * turned[8 * q : 8 * q + STEP]
        pad[aligned(i, STEP), :] = total
        lane = lax.broadcasted_iota(jnp.int32, (STEP, 128), 1)
        plain = jnp.sum(total, axis=1, keepdims=True)
        square = jnp.sum(total * total, axis=1, keepdims=True)
        cols_st[aligned(i, STEP), :] = jnp.where(
            lane == 0, plain, jnp.where(lane == 1, square, 0.0)
        )

    stat[0] = cols_st[...].T[:8]
    stat_near = remote(stat.at[0], stat.at[1], stat_sem.at[0], stat_sem.at[1], near)
    stat_near.start()
    stat_near.wait()
    stat[2] = stat[0] + stat[1]
    stat_far = remote(stat.at[2], stat.at[3], stat_sem.at[2], stat_sem.at[3], far)
    stat_far.start()
    up_far.start()
    for c in range(CHUNKS):
        down_far[c].start()
    up_near.start()
    for c in range(CHUNKS):
        down_near[c].start()

    @pl.loop(1, 4)
    def _(j):
        normalize(lax.rem(t + j, 4))

    get_sg.wait()
    get_su.wait()
    sacc[...] = jnp.zeros_like(sacc)

    @pl.loop(0, CHUNKS)
    def _(k):
        at = aligned(k, chunk)
        sacc[0] += dot(tok[:, at], wbuf[0, at, :])
        sacc[1] += dot(tok[:, at], wbuf[4, at, :])

    get_own_gate = fetch(expert_gate, wbuf.at[0], 3)
    get_own_up = fetch(expert_up, wbuf.at[4], 4)
    get_own_gate.start()
    get_own_up.start()
    hs[...] = (silu(sacc[0]) * sacc[1]).astype(BF16)

    def halves(which, lhs, depth):
        @pl.loop(0, width // TILE)
        def _(i):
            at = aligned(i, TILE)
            for j in range(2):
                block = aligned(2 * j + 1 - core, own)
                ns[j, :, at] = dot(lhs[block, :], opbuf[pl.ds(0, depth), at]).astype(BF16)
            for j in range(2):
                block = aligned(2 * j + core, own)
                kept[which, j, :, at] = dot(lhs[block, :], opbuf[pl.ds(0, depth), at]).astype(BF16)

    to_near = [
        remote(ns, nr.at[which], rs_near.at[which, 0], rs_near.at[which, 1], near) for which in range(2)
    ]
    crossing = [
        remote(kept.at[which, 1 - low], arr.at[which], rs_far.at[which, 0], rs_far.at[which, 1], far)
        for which in range(2)
    ]

    def cross(which):
        to_near[which].wait_recv()

        @pl.loop(0, own // 16)
        def _(i):
            at = aligned(i, 16)
            kept[which, 1 - low, at, :] = (
                kept[which, 1 - low, at, :].astype(F32) + nr[which, 1 - low, at, :].astype(F32)
            ).astype(BF16)

        crossing[which].start()

    get_sd.wait()
    halves(0, hs, hidden)
    to_near[0].start()
    get_op = fetch(out_proj, opbuf, 5)
    get_op.start()

    stat_far.wait()
    cross(0)
    total = stat[2] + stat[3]
    cols_st[...] = jnp.concatenate([total, jnp.zeros((120, length), F32)], axis=0).T
    channels = pad.shape[1] * 4

    @pl.loop(0, length // STEP)
    def _(i):
        at = aligned(i, STEP)
        average = cols_st[at, 0:1] / channels
        variance = cols_st[at, 1:2] / channels - average * average
        scale = lax.rsqrt(variance + EPSILON)
        v = (pad[at, :] - average) * scale * ln_gain[...] + ln_bias[...]
        act[at, :] = silu(v).astype(BF16)

    gate_far.wait()
    gate_on.start()
    get_op.wait()
    to_near[0].wait_send()
    halves(1, act, act.shape[1])
    to_near[1].start()
    get_down = fetch(expert_down, opbuf.at[pl.ds(0, hidden)], 6)
    get_down.start()
    cross(1)

    for c in range(CHUNKS):

        @pl.loop(1, count)
        def _(j):
            source = lax.rem(me + j, count)
            remote(
                box.at[c, source],
                rows.at[c, source],
                go_send.at[c, source],
                go_recv.at[c, source],
                {"ep": source},
            ).wait()

    def product(into, slot):
        into[...] = jnp.zeros(into.shape, F32)

        @pl.loop(0, CHUNKS)
        def _(k):
            into[...] += dot(rows[k].reshape(slots, chunk), wbuf[slot, aligned(k, chunk), :])

    def finish(piece):
        product(sacc.at[0, pl.ds(0, slots)], piece + 4)
        hid[piece] = (silu(gacc[piece]) * sacc[0, pl.ds(0, slots), :]).astype(BF16)

    get_own_gate.wait()
    product(gacc.at[0], 0)
    gate_near.wait()
    product(gacc.at[2], 2)
    product(gacc.at[1], 1)
    gate_on.wait()
    product(gacc.at[3], 3)
    get_own_up.wait()
    finish(0)
    up_near.wait()
    finish(2)
    up_far.wait()
    up_on.start()
    finish(1)
    up_on.wait()
    finish(3)
    get_down.wait()

    def back(c, j):
        to = lax.rem(me + j, count)
        return remote(box.at[c, to], ret.at[c, me], ret_send.at[c, to], ret_recv.at[c, me], {"ep": to})

    for c in range(CHUNKS):
        down_far[c].wait()
        down_on[c].start()
        down_near[c].wait()
        down_on[c].wait()

        @pl.loop(0, chunk // TILE)
        def _(i):
            at = pl.ds(pl.multiple_of(c * chunk + i * TILE, TILE), TILE)
            total = dot(hid[0], opbuf[pl.ds(0, hidden), at])
            for piece in range(3):
                total += dot(hid[piece + 1], downs[piece, :, at])
            box[c, :, :, aligned(i, TILE)] = total.astype(BF16).reshape(count, cap, TILE)

        @pl.loop(1, count)
        def _(j):
            back(c, j).start()

        ret[c, me] = box[c, me]

    def ended(which, at):
        return (
            kept[which, low, :, at].astype(F32)
            + nr[which, low, :, at].astype(F32)
            + arr[which, :, at].astype(F32)
        ).astype(BF16)

    def put(which, at, into, i):
        return pltpu.make_async_copy(arr.at[which, :, at], into.at[:, at], put_sem.at[i])

    crossing[0].wait()
    for c in range(CHUNKS):

        @pl.loop(1, count)
        def _(j):
            source = lax.rem(me + j, count)
            remote(
                box.at[c, source],
                ret.at[c, source],
                ret_send.at[c, source],
                ret_recv.at[c, source],
                {"ep": source},
            ).wait()

        @pl.loop(0, chunk // TILE)
        def _(i):
            at = pl.ds(pl.multiple_of(c * chunk + i * TILE, TILE), TILE)
            total = ended(0, at).astype(F32)
            came = ret[c, :, :, aligned(i, TILE)].reshape(slots, TILE)
            for k in range(choice.shape[0]):
                total += dot(choice[k], came) * share[:, k : k + 1]
            arr[0, :, at] = total.astype(BF16)

        put(0, cols(c), out_ref, c).start()

    to_near[1].wait_send()
    crossing[1].wait()

    @pl.loop(0, width // TILE)
    def _(i):
        at = aligned(i, TILE)
        arr[1, :, at] = ended(1, at)

    put(1, pl.ds(0, width), mixer_ref, CHUNKS).start()
    for c in range(CHUNKS):
        put(0, cols(c), out_ref, c).wait()
    put(1, pl.ds(0, width), mixer_ref, CHUNKS).wait()


def per_device(
    value_in,
    gate_in,
    conv_taps,
    conv_bias,
    ln_gain,
    ln_bias,
    out_proj,
    tokens_b,
    norm_gain,
    routes,
    route_weights,
    expert_gate,
    expert_up,
    expert_down,
    shared_gate,
    shared_up,
    shared_down,
):
    ep_count = lax.axis_size("ep")
    own, top_count = routes.shape
    length, channels = value_in.shape
    width, hidden = tokens_b.shape[1], expert_down.shape[1]
    cap = 3 * own * top_count // (2 * ep_count)
    cap = -(-cap // 16) * 16
    slots, chunk = ep_count * cap, width // CHUNKS
    anywhere = pl.BlockSpec(memory_space=pl.ANY)
    vmem = pl.BlockSpec(memory_space=pltpu.VMEM)
    dma = pltpu.SemaphoreType.DMA
    mail = pltpu.VMEM((CHUNKS, ep_count, cap, chunk), BF16)
    return pl.pallas_call(
        kernel,
        out_shape=[jax.ShapeDtypeStruct((own, width), BF16)] * 2,
        in_specs=[vmem] * 9 + [anywhere] * 8,
        out_specs=[anywhere, anywhere],
        scratch_shapes=[
            pltpu.VMEM((8, width, hidden), BF16),
            pltpu.VMEM((max(channels, hidden), width), BF16),
            pltpu.VMEM((3, hidden, width), BF16),
            pltpu.VMEM((4 * own, width), BF16),
            mail,
            mail,
            mail,
            pltpu.VMEM((length + RIM, channels), F32),
            pltpu.VMEM((length, channels), BF16),
            pltpu.VMEM((4 * own, hidden), BF16),
            pltpu.VMEM((2, own, width), BF16),
            pltpu.VMEM((2, 2, own, width), BF16),
            pltpu.VMEM((2, 2, own, width), BF16),
            pltpu.VMEM((2, own, width), BF16),
            pltpu.VMEM((2, 4 * own, hidden), F32),
            pltpu.VMEM((4, slots, hidden), F32),
            pltpu.VMEM((4, slots, hidden), BF16),
            pltpu.VMEM((4, 8, length), F32),
            pltpu.VMEM((length, 128), F32),
            pltpu.VMEM((top_count, own, slots), BF16),
            dma((7,)),
            dma((CHUNKS + 1,)),
            dma((4,)),
            dma((2,)),
            dma((4,)),
            dma((6,)),
            dma((6,)),
            dma((CHUNKS,)),
            dma((CHUNKS,)),
            dma((2, CHUNKS)),
            dma((2, CHUNKS)),
            dma((2, 2)),
            dma((2, 2)),
            dma((CHUNKS, ep_count)),
            dma((CHUNKS, ep_count)),
            dma((CHUNKS, ep_count)),
            dma((CHUNKS, ep_count)),
        ],
        compiler_params=pltpu.CompilerParams(
            collective_id=0, has_side_effects=True, vmem_limit_bytes=67043328
        ),
    )(
        value_in,
        gate_in,
        conv_taps,
        conv_bias[None],
        ln_gain[None],
        ln_bias[None],
        norm_gain[None],
        routes,
        route_weights,
        out_proj,
        tokens_b,
        expert_gate[0],
        expert_up[0],
        expert_down[0],
        shared_gate,
        shared_up,
        shared_down,
    )


def solution(mesh):
    return jax.shard_map(
        lambda *args: tuple(per_device(*args)),
        mesh=mesh,
        in_specs=(
            P("ep", "tp"),
            P("ep", "tp"),
            P(None, "tp"),
            P("tp"),
            P("tp"),
            P("tp"),
            P("tp", None),
            P("ep", None),
            P(),
            P(("ep", "tp"), None),
            P(("ep", "tp"), None),
            P("ep", None, "tp"),
            P("ep", None, "tp"),
            P("ep", "tp", None),
            P(None, "tp"),
            P(None, "tp"),
            P("tp", None),
        ),
        out_specs=(P(("ep", "tp"), None), P(("ep", "tp"), None)),
        check_vma=False,
    )
```

time: 237 us -> 200 us (0.84)
  Pallas kernels: 0 us -> 189 us
  waiting for transfers between devices: 85.1 us -> 0 us
  matrix products: 63 us -> 0 us
  starting transfers between devices: 30.6 us -> 0 us
  blocking collectives: 26.3 us -> 0 us
  other arithmetic: 23.2 us -> 0 us
  local copies, waits for them, and re-layouts: 3.3 us -> 6.18 us
    pallas_call x0 -> x1, Pallas kernels: none -> 189 us  [per_device(): pl.pallas_call(kernel, out_shape=[jax.ShapeDtypeStruct((own, width), BF16...]
    ppermute x17 -> x0, waiting for transfers between devices: 85.1 us -> none  [the longest x1 49.5 us: shifted(): return lax.ppermute(x, axis, pairs)]
    dot_general x28 -> x0, matrix products: 63 us -> none  [the longest x5 17.3 us: gated_hidden(): jnp.dot(rows_in, weight_gate, preferred_element_type=jnp.float32)]
    psum x1 -> x0, blocking collectives: 26.3 us -> none  [per_device(): row_sum, squares = lax.psum((row_sum, squares), 'tp')]
    all_to_all x3 -> x0, starting transfers between devices: 18.7 us -> none  [the longest x2 12.4 us: per_device(): lax.all_to_all(product.reshape(ep_count, capacity, chunk), 'ep', split_ax...]
    ppermute x17 -> x0, starting transfers between devices: 11.9 us -> none  [the longest x16 8.56 us: swapped(): return lax.ppermute(x, axis, [(i, i ^ bit) for i in range(devices)])]
    convert_element_type x7 -> x0, other arithmetic: 10.8 us -> none  [the longest x2 3.51 us: scattered_product(): give = sum((g.astype(jnp.float32) for g in give)).astype(jnp.bfloat16)]
    reduce_sum x3 -> x0, other arithmetic: 10.4 us -> none  [the longest x1 5.7 us: per_device(): jnp.sum(filtered * filtered, axis=1)]
  transfers between devices with their start and end apart: 20 -> 0, of which waited for: 4 -> 0; matrix products, arithmetic and copies ran while one was open for 36% -> 0% of each run, Pallas kernels for 0% -> 0%
where the time goes in v2:
time: 200 us; the launch traced here: 196 us
  Pallas kernels  189 us (94%)
  local copies, waits for them, and re-layouts  6.18 us (3%)
    pallas_call x1, Pallas kernels, per_device(): pl.pallas_call(kernel, out_shape=[jax.ShapeDtypeStruct((own, width), BF16...  189 us
    unnamed x6, local copies, waits for them, and re-layouts  6.18 us

profile of v2, /device:TPU:12, one launch (start us, length us, event | category | flops | bytes accessed | tf_op | source)
XLA Modules:
  0.0 196.1 jit_solution(2311342315979016897)
XLA Ops:
  0.6 1.4 copy.19.routes
  2.0 1.4 copy.20.share
  3.5 189.3 %shard_map.176 = (bf16[128,4096]{1,0:T(8,128)(2,1)}, bf16[128,4096]{1,0:T(8,128)(2,1)}) custom-call(bf16[512,512]{1,0:T(8,128)(2,1)} %value.1, bf16[512,512]{1,0:T(8,128)(2,1)} %gate.1, f32[31,512]{1,0:T(8,128)} %taps.1, f32[1,512]{1,0:T(1,128)} %bitcast.11, f32[1,512]{1,0:T(1,128)} %bitcast.12, f32[1,512]{1,0:T(1,128)} %bitcast.13, f32[1,4096]{1,0:T(1,128)} %bitcast.10, ...), custom_call_target="tpu_custom_call" | custom-call | tf_op jit(solution)/shard_map/pallas_call | solution.py:503
  192.8 0.0 copy-start
  192.8 2.4 %copy.23 = bf16[128,4096]{1,0:T(8,128)(2,1)} copy(bf16[128,4096]{1,0:T(8,128)(2,1)} %get-tuple-element.4) | data formatting | bytes 2097152
  195.2 0.0 copy-done
  195.2 1.0 copy.24
Async XLA Ops:
  192.8 2.4 %copy-start = (bf16[128,4096]{1,0:T(8,128)(2,1)S(1)}, bf16[128,4096]{1,0:T(8,128)(2,1)}, u32[]{:S(2)}) copy-start(bf16[128,4096]{1,0:T(8,128)(2,1)} %get-tuple-element.5) | copy-start | bytes 3145732

commit v3 on v2

v3 whole, which is shorter than its diff:
```python
import jax
import jax.numpy as jnp
from jax import lax
from jax.experimental import pallas as pl
from jax.experimental.pallas import tpu as pltpu
from jax.sharding import PartitionSpec as P

MESH = pl.DeviceIdType.MESH
EPSILON = 1e-06
CHUNKS = 4
TILE = 256
STEP = 32
UNIT = 16
RIM = 32
F32, BF16 = jnp.float32, jnp.bfloat16


def dot(a, b):
    return jnp.dot(a, b, preferred_element_type=F32)


def silu(v):
    return v * jax.nn.sigmoid(v)


def aligned(i, size):
    return pl.ds(pl.multiple_of(i * size, size), size)


def kernel(
    value,
    gate,
    taps,
    bias,
    ln_gain,
    ln_bias,
    norm_gain,
    routes,
    share,
    out_proj,
    tokens,
    expert_gate,
    expert_up,
    expert_down,
    shared_gate,
    shared_up,
    shared_down,
    mixer_ref,
    out_ref,
    wbuf,
    opbuf,
    dbuf,
    downs,
    tok,
    box,
    dup,
    rows,
    frows,
    ret,
    pad,
    act,
    hs,
    ns,
    kept,
    nr,
    arr,
    sacc,
    hid,
    hfar,
    total_out,
    stat,
    cols_st,
    choice,
    share_cols,
    froutes,
    load,
    put_sem,
    tok_load,
    halo_sem,
    stat_sem,
    route_sem,
    w_send,
    w_recv,
    down_send,
    down_recv,
    near_send,
    near_recv,
    rs_near,
    rs_far,
    go_send,
    go_recv,
    dup_send,
    dup_recv,
    f_send,
    f_recv,
    h_send,
    h_recv,
    ret_send,
    ret_recv,
):
    me, t = lax.axis_index("ep"), lax.axis_index("tp")
    count = lax.axis_size("ep")
    groups = box.shape[0]
    own = share.shape[1]
    length, width = value.shape[0], tok.shape[1]
    chunk = width // CHUNKS
    batch = count * UNIT
    core, low = lax.rem(t, 2), t // 2
    near = {"tp": t + 1 - 2 * core}
    far = {"tp": lax.rem(t + 2, 4)}
    far_t = lax.rem(t + 2, 4)
    base = (me // 2) * 2
    partner = base + 1 - lax.rem(me, 2)
    hidden = hs.shape[1]
    tiles = width // TILE

    def remote(src, dst, send, recv, to):
        return pltpu.make_async_remote_copy(
            src_ref=src, dst_ref=dst, send_sem=send, recv_sem=recv, device_id=to, device_id_type=MESH
        )

    def fetch(src, dst, i):
        return pltpu.make_async_copy(src, dst, load.at[i])

    def cols(c):
        return pl.ds(c * chunk, chunk)

    barrier = pltpu.get_barrier_semaphore()
    pl.semaphore_signal(barrier, inc=1, device_id=near, device_id_type=MESH)
    pl.semaphore_signal(barrier, inc=1, device_id=far, device_id_type=MESH)

    @pl.loop(1, count)
    def _(j):
        pl.semaphore_signal(
            barrier, inc=1, device_id={"ep": lax.rem(me + j, count)}, device_id_type=MESH
        )

    def tokens_load(b):
        return pltpu.make_async_copy(tokens.at[aligned(b, own)], tok.at[aligned(b, own)], tok_load.at[b])

    tokens_load(t).start()
    tokens_load(far_t).start()
    get_sg = fetch(shared_gate, wbuf.at[0], 0)
    get_su = fetch(shared_up, wbuf.at[2], 1)
    get_sd = fetch(shared_down, opbuf.at[pl.ds(0, hidden)], 2)
    get_down = fetch(expert_down, dbuf, 6)
    get_sg.start()
    get_su.start()
    tokens_load(lax.rem(t + 1, 4)).start()
    tokens_load(lax.rem(t + 3, 4)).start()
    get_sd.start()
    get_down.start()
    pl.semaphore_wait(barrier, count + 1)

    routes_far = remote(routes, froutes, route_sem.at[0], route_sem.at[1], far)
    gate_near = remote(expert_gate, wbuf.at[1], w_send.at[0], w_recv.at[0], near)
    up_near = remote(expert_up, wbuf.at[3], w_send.at[1], w_recv.at[1], near)
    down_far = [
        remote(expert_down.at[:, cols(c)], downs.at[0, :, cols(c)], down_send.at[c], down_recv.at[c], far)
        for c in range(CHUNKS)
    ]
    down_near = [
        remote(
            expert_down.at[:, cols(c)],
            downs.at[1, :, cols(c)],
            near_send.at[0, c],
            near_recv.at[0, c],
            near,
        )
        for c in range(CHUNKS)
    ]
    down_on = [
        remote(
            downs.at[0, :, cols(c)],
            downs.at[2, :, cols(c)],
            near_send.at[1, c],
            near_recv.at[1, c],
            near,
        )
        for c in range(CHUNKS)
    ]
    routes_far.start()
    down_far[0].start()
    down_far[1].start()
    gate_near.start()
    up_near.start()
    for c in range(CHUNKS):
        down_near[c].start()

    @pl.loop(0, length // STEP)
    def _(i):
        at = aligned(i, STEP)
        gated = value[at, :].astype(F32) * jax.nn.sigmoid(gate[at, :].astype(F32))
        pad[aligned(i + 1, STEP), :] = gated.astype(BF16).astype(F32)

    def halo(to):
        return remote(
            pad.at[pl.ds(length, RIM)], pad.at[pl.ds(0, RIM)], halo_sem.at[0], halo_sem.at[1], {"ep": to}
        )

    @pl.when(me < count - 1)
    def _():
        halo(lax.rem(me + 1, count)).start()

    @pl.when(me == 0)
    def _():
        pad[pl.ds(0, RIM), :] = jnp.zeros((RIM, pad.shape[1]), F32)

    def normalize(b):
        tokens_load(b).wait()

        @pl.loop(0, own // 16)
        def _(i):
            at = pl.ds(pl.multiple_of(b * own + i * 16, 16), 16)
            x = tok[at, :].astype(F32)
            scale = lax.rsqrt(jnp.mean(x * x, axis=1, keepdims=True) + EPSILON)
            tok[at, :] = (x * scale * norm_gain[...]).astype(BF16)

    def tall(wide):
        return jnp.concatenate([wide, jnp.zeros((own - wide.shape[0], own), F32)], axis=0).T

    def placed(ids):
        lanes = lax.broadcasted_iota(jnp.int32, (own, own), 1).astype(F32)
        columns = tall(ids.astype(F32))
        chosen = [columns[:, k : k + 1] for k in range(ids.shape[0])]
        names = [(lanes == r).astype(F32) for r in chosen]
        before = lax.broadcasted_iota(jnp.int32, (own, own), 1) < lax.broadcasted_iota(
            jnp.int32, (own, own), 0
        )
        earlier = dot(before.astype(F32).astype(BF16), sum(names).astype(BF16))
        return [
            (r, jnp.sum(earlier * name, axis=1, keepdims=True)) for r, name in zip(chosen, names)
        ]

    normalize(t)
    share_cols[...] = tall(share[...])
    places = lax.broadcasted_iota(jnp.int32, (own, groups * batch), 1).astype(F32)
    anywhere = jnp.zeros((own, groups * batch), F32)
    for k, (r, place) in enumerate(placed(routes[...])):
        spot = place + UNIT * (r + (count - 1) * jnp.floor(place * (1 / UNIT)))
        chosen = (places == spot).astype(F32)
        anywhere = anywhere + chosen
        for g in range(groups):
            choice[k, g] = chosen[:, g * batch : (g + 1) * batch].astype(BF16)
    pick = anywhere.T.astype(BF16)

    def going(g, to):
        return remote(box.at[g, to], rows.at[g, me], go_send.at[g, to], go_recv.at[g, me], {"ep": to})

    def came(g, source):
        return remote(
            box.at[g, source], rows.at[g, source], go_send.at[g, source], go_recv.at[g, source], {"ep": source}
        )

    for g in range(groups):
        part = pick[g * batch : (g + 1) * batch]

        @pl.loop(0, tiles)
        def _(i):
            at = aligned(i, TILE)
            box[g, :, :, at] = dot(part, tok[aligned(t, own), at]).astype(BF16).reshape(count, UNIT, TILE)

        @pl.loop(1, count)
        def _(j):
            going(g, lax.rem(me + j, count)).start()

        rows[g, me] = box[g, me]

    normalize(far_t)
    routes_far.wait()
    spots = lax.broadcasted_iota(jnp.int32, (own, own), 1).astype(F32)
    anywhere = jnp.zeros((own, own), F32)
    first_of_pair = base.astype(F32)
    for r, place in placed(froutes[...]):
        inside = (r - first_of_pair >= 0) & (r - first_of_pair <= 1)
        spot = place + UNIT * (r - first_of_pair + jnp.floor(place * (1 / UNIT)))
        anywhere = anywhere + jnp.where(inside & (spots == spot), 1.0, 0.0)
    pick = anywhere.T.astype(BF16)[: groups * 2 * UNIT]

    @pl.loop(0, tiles)
    def _(i):
        at = aligned(i, TILE)
        dup[:, :, :, at] = (
            dot(pick, tok[aligned(far_t, own), at]).astype(BF16).reshape(groups, 2, UNIT, TILE)
        )

    doubles = [
        remote(
            dup.at[g, partner - base], frows.at[g, me], dup_send.at[g], dup_recv.at[g], {"ep": partner}
        )
        for g in range(groups)
    ]
    for g in range(groups):
        doubles[g].start()
        frows[g, me] = dup[g, me - base]

    @pl.when(me < count - 1)
    def _():
        halo(lax.rem(me + 1, count)).wait_send()

    @pl.when(me > 0)
    def _():
        halo(lax.rem(me + 1, count)).wait_recv()

    tap_count = taps.shape[0]
    first = RIM - (tap_count - 1)

    @pl.loop(0, length // STEP)
    def _(i):
        window = pad[pl.ds(pl.multiple_of(i * STEP, STEP), STEP + RIM), :]
        total = jnp.zeros((STEP, window.shape[1]), F32) + bias[...]
        for s in range(8):
            turned = pltpu.roll(window, STEP + RIM - s, 0) if s else window
            for q in range((RIM + 8) // 8):
                j = s + 8 * q - first
                if 0 <= j < tap_count:
                    total = total + taps[j : j + 1, :] * turned[8 * q : 8 * q + STEP]
        pad[aligned(i, STEP), :] = total
        lane = lax.broadcasted_iota(jnp.int32, (STEP, 128), 1)
        plain = jnp.sum(total, axis=1, keepdims=True)
        square = jnp.sum(total * total, axis=1, keepdims=True)
        cols_st[aligned(i, STEP), :] = jnp.where(
            lane == 0, plain, jnp.where(lane == 1, square, 0.0)
        )

    stat[0] = cols_st[...].T[:8]
    stat_near = remote(stat.at[0], stat.at[1], stat_sem.at[0], stat_sem.at[1], near)
    stat_near.start()

    normalize(lax.rem(t + 1, 4))
    normalize(lax.rem(t + 3, 4))
    stat_near.wait()
    stat[2] = stat[0] + stat[1]
    stat_far = remote(stat.at[2], stat.at[3], stat_sem.at[2], stat_sem.at[3], far)
    stat_far.start()
    get_sg.wait()
    get_su.wait()
    sacc[...] = jnp.zeros_like(sacc)

    @pl.loop(0, CHUNKS)
    def _(k):
        at = aligned(k, chunk)
        sacc[0] += dot(tok[:, at], wbuf[0, at, :])
        sacc[1] += dot(tok[:, at], wbuf[2, at, :])

    get_own_gate = fetch(expert_gate, wbuf.at[0], 3)
    get_own_up = fetch(expert_up, wbuf.at[2], 4)
    get_own_gate.start()
    get_own_up.start()
    hs[...] = (silu(sacc[0]) * sacc[1]).astype(BF16)

    def outside(j):
        return lax.rem(base + 2 + j, count)

    def forward(g, source):
        return remote(
            rows.at[g, source], frows.at[g, source], f_send.at[g, source], f_recv.at[g, source], far
        )

    def forward_group(g):
        @pl.loop(0, count - 2)
        def _(j):
            came(g, outside(j)).wait_recv()
            forward(g, outside(j)).start()

        came(g, partner).wait_recv()

    def far_ready(g):
        doubles[g].wait_recv()

        @pl.loop(0, count - 2)
        def _(j):
            forward(g, outside(j)).wait()

    def ffn(source, g, slot):
        lhs = source.at[g]
        gate_sum = jnp.zeros((batch, hidden), F32)
        up_sum = jnp.zeros((batch, hidden), F32)

        def step(k, sums):
            at = aligned(k, chunk)
            x = lhs[:, :, at].reshape(batch, chunk)
            return sums[0] + dot(x, wbuf[slot, at, :]), sums[1] + dot(x, wbuf[slot + 2, at, :])

        gate_sum, up_sum = lax.fori_loop(0, CHUNKS, step, (gate_sum, up_sum))
        return (silu(gate_sum) * up_sum).astype(BF16)

    def own_part(g):
        hid[g, 0] = ffn(rows, g, 0)
        hid[g, 2] = ffn(rows, g, 1)

    hidden_far = [
        [
            remote(hfar.at[g, n], hid.at[g, 1 + 2 * n], h_send.at[g, n], h_recv.at[g, n], far)
            for n in range(2)
        ]
        for g in range(groups)
    ]

    def far_part(g):
        far_ready(g)
        for n in range(2):
            hfar[g, n] = ffn(frows, g, n)
            hidden_far[g][n].start()

    def halves(which, lhs, depth):
        @pl.loop(0, tiles)
        def _(i):
            at = aligned(i, TILE)
            for j in range(2):
                block = aligned(2 * j + 1 - core, own)
                ns[j, :, at] = dot(lhs[block, :], opbuf[pl.ds(0, depth), at]).astype(BF16)
            for j in range(2):
                block = aligned(2 * j + core, own)
                kept[which, j, :, at] = dot(lhs[block, :], opbuf[pl.ds(0, depth), at]).astype(BF16)

    to_near = [
        remote(ns, nr.at[which], rs_near.at[which, 0], rs_near.at[which, 1], near) for which in range(2)
    ]
    crossing = [
        remote(kept.at[which, 1 - low], arr.at[which], rs_far.at[which, 0], rs_far.at[which, 1], far)
        for which in range(2)
    ]

    def joined(which):
        to_near[which].wait_recv()

        @pl.loop(0, own // 16)
        def _(i):
            at = aligned(i, 16)
            kept[which, 1 - low, at, :] = (
                kept[which, 1 - low, at, :].astype(F32) + nr[which, 1 - low, at, :].astype(F32)
            ).astype(BF16)

    def back(g, to):
        return remote(box.at[g, to], ret.at[g, me], ret_send.at[g, to], ret_recv.at[g, me], {"ep": to})

    def products(g):
        @pl.loop(1, count)
        def _(j):
            came(g, lax.rem(me + j, count)).wait_send()

        for n in range(2):
            hidden_far[g][n].wait()

        @pl.loop(0, tiles)
        def _(i):
            at = aligned(i, TILE)
            total = dot(hid[g, 0], dbuf[:, at])
            for piece in range(3):
                total += dot(hid[g, piece + 1], downs[piece, :, at])
            box[g, :, :, at] = total.astype(BF16).reshape(count, UNIT, TILE)

        @pl.loop(1, count)
        def _(j):
            back(g, lax.rem(me + j, count)).start()

        ret[g, me] = box[g, me]

    def combine(g):
        @pl.loop(1, count)
        def _(j):
            source = lax.rem(me + j, count)
            remote(
                box.at[g, source],
                ret.at[g, source],
                ret_send.at[g, source],
                ret_recv.at[g, source],
                {"ep": source},
            ).wait()

        @pl.loop(0, tiles)
        def _(i):
            at = aligned(i, TILE)
            back_rows = ret[g, :, :, at].reshape(batch, TILE)
            total = jnp.zeros((own, TILE), F32)
            for k in range(choice.shape[0]):
                total += dot(choice[k, g], back_rows) * share_cols[:, k : k + 1]
            if g:
                total += total_out[:, at]
            if g == groups - 1:
                arr[0, :, at] = (total + ended(0, at).astype(F32)).astype(BF16)
            else:
                total_out[:, at] = total

    def ended(which, at):
        return (
            kept[which, low, :, at].astype(F32)
            + nr[which, low, :, at].astype(F32)
            + arr[which, :, at].astype(F32)
        ).astype(BF16)

    def put(which, into):
        return pltpu.make_async_copy(arr.at[which], into, put_sem.at[which])

    def normed():
        stat_far.wait()
        total = stat[2] + stat[3]
        cols_st[...] = jnp.concatenate([total, jnp.zeros((120, length), F32)], axis=0).T
        channels = pad.shape[1] * 4

        @pl.loop(0, length // STEP)
        def _(i):
            at = aligned(i, STEP)
            average = cols_st[at, 0:1] / channels
            variance = cols_st[at, 1:2] / channels - average * average
            scale = lax.rsqrt(variance + EPSILON)
            v = (pad[at, :] - average) * scale * ln_gain[...] + ln_bias[...]
            act[at, :] = silu(v).astype(BF16)

    def relay(c):
        down_far[c].wait()
        down_on[c].start()

    get_op = fetch(out_proj, opbuf, 5)

    forward_group(0)
    down_far[2].start()
    down_far[3].start()
    relay(0)
    relay(1)
    get_own_gate.wait()
    get_own_up.wait()
    gate_near.wait()
    up_near.wait()
    own_part(0)
    get_sd.wait()
    halves(0, hs, hidden)
    to_near[0].start()
    get_op.start()
    far_part(0)
    normed()
    if groups > 1:
        forward_group(1)
        own_part(1)
    get_op.wait()
    to_near[0].wait_send()
    halves(1, act, act.shape[1])
    to_near[1].start()
    joined(0)
    relay(2)
    relay(3)
    get_down.wait()
    for c in range(CHUNKS):
        down_near[c].wait()
        down_on[c].wait()
    products(0)
    for g in range(1, groups):
        if g > 1:
            forward_group(g)
            own_part(g)
    joined(1)
    for g in range(1, groups):
        far_part(g)
    crossing[0].start()
    crossing[1].start()
    for g in range(1, groups):
        products(g)
    for g in range(groups - 1):
        combine(g)
    for g in range(groups):
        doubles[g].wait_send()
    to_near[1].wait_send()
    crossing[0].wait()
    combine(groups - 1)
    put(0, out_ref).start()
    crossing[1].wait()

    @pl.loop(0, tiles)
    def _(i):
        at = aligned(i, TILE)
        arr[1, :, at] = ended(1, at)

    put(1, mixer_ref).start()
    put(0, out_ref).wait()
    put(1, mixer_ref).wait()


def per_device(
    value_in,
    gate_in,
    conv_taps,
    conv_bias,
    ln_gain,
    ln_bias,
    out_proj,
    tokens_b,
    norm_gain,
    routes,
    route_weights,
    expert_gate,
    expert_up,
    expert_down,
    shared_gate,
    shared_up,
    shared_down,
):
    ep_count = lax.axis_size("ep")
    own, top_count = routes.shape
    length, channels = value_in.shape
    width, hidden = tokens_b.shape[1], expert_down.shape[1]
    cap = 3 * own * top_count // (2 * ep_count)
    groups = -(-cap // UNIT)
    batch = ep_count * UNIT
    anywhere = pl.BlockSpec(memory_space=pl.ANY)
    vmem = pl.BlockSpec(memory_space=pltpu.VMEM)
    dma = pltpu.SemaphoreType.DMA
    mail = pltpu.VMEM((groups, ep_count, UNIT, width), BF16)
    return pl.pallas_call(
        kernel,
        out_shape=[jax.ShapeDtypeStruct((own, width), BF16)] * 2,
        in_specs=[vmem] * 9 + [anywhere] * 8,
        out_specs=[anywhere, anywhere],
        scratch_shapes=[
            pltpu.VMEM((4, width, hidden), BF16),
            pltpu.VMEM((max(channels, hidden), width), BF16),
            pltpu.VMEM((hidden, width), BF16),
            pltpu.VMEM((3, hidden, width), BF16),
            pltpu.VMEM((4 * own, width), BF16),
            mail,
            pltpu.VMEM((groups, 2, UNIT, width), BF16),
            mail,
            mail,
            mail,
            pltpu.VMEM((length + RIM, channels), F32),
            pltpu.VMEM((length, channels), BF16),
            pltpu.VMEM((4 * own, hidden), BF16),
            pltpu.VMEM((2, own, width), BF16),
            pltpu.VMEM((2, 2, own, width), BF16),
            pltpu.VMEM((2, 2, own, width), BF16),
            pltpu.VMEM((2, own, width), BF16),
            pltpu.VMEM((2, 4 * own, hidden), F32),
            pltpu.VMEM((groups, 4, batch, hidden), BF16),
            pltpu.VMEM((groups, 2, batch, hidden), BF16),
            pltpu.VMEM((own, width), F32),
            pltpu.VMEM((4, 8, length), F32),
            pltpu.VMEM((length, 128), F32),
            pltpu.VMEM((top_count, groups, own, batch), BF16),
            pltpu.VMEM((own, own), F32),
            pltpu.VMEM((top_count, own), jnp.int32),
            dma((7,)),
            dma((2,)),
            dma((4,)),
            dma((2,)),
            dma((4,)),
            dma((2,)),
            dma((2,)),
            dma((2,)),
            dma((CHUNKS,)),
            dma((CHUNKS,)),
            dma((2, CHUNKS)),
            dma((2, CHUNKS)),
            dma((2, 2)),
            dma((2, 2)),
            dma((groups, ep_count)),
            dma((groups, ep_count)),
            dma((groups,)),
            dma((groups,)),
            dma((groups, ep_count)),
            dma((groups, ep_count)),
            dma((groups, 2)),
            dma((groups, 2)),
            dma((groups, ep_count)),
            dma((groups, ep_count)),
        ],
        compiler_params=pltpu.CompilerParams(
            collective_id=0, has_side_effects=True, vmem_limit_bytes=67043328
        ),
    )(
        value_in,
        gate_in,
        conv_taps,
        conv_bias[None],
        ln_gain[None],
        ln_bias[None],
        norm_gain[None],
        routes.T,
        route_weights.T,
        out_proj,
        tokens_b,
        expert_gate[0],
        expert_up[0],
        expert_down[0],
        shared_gate,
        shared_up,
        shared_down,
    )


def solution(mesh):
    return jax.shard_map(
        lambda *args: tuple(per_device(*args)),
        mesh=mesh,
        in_specs=(
            P("ep", "tp"),
            P("ep", "tp"),
            P(None, "tp"),
            P("tp"),
            P("tp"),
            P("tp"),
            P("tp", None),
            P("ep", None),
            P(),
            P(("ep", "tp"), None),
            P(("ep", "tp"), None),
            P("ep", None, "tp"),
            P("ep", None, "tp"),
            P("ep", "tp", None),
            P(None, "tp"),
            P(None, "tp"),
            P("tp", None),
        ),
        out_specs=(P(("ep", "tp"), None), P(("ep", "tp"), None)),
        check_vma=False,
    )
```

time: 200 us -> 182 us (0.910); the launches traced: 196 us -> 181 us
  Pallas kernels: 189 us -> 177 us
  local copies, waits for them, and re-layouts: 6.18 us -> 3.35 us
    pallas_call x1, Pallas kernels: 189 us -> 177 us  [per_device(): pl.pallas_call(kernel, out_shape=[jax.ShapeDtypeStruct((own, width), BF16...]
    unnamed x6 -> x4, local copies, waits for them, and re-layouts: 6.18 us -> 3.35 us
where the time goes in v3:
time: 182 us; the launch traced here: 181 us
  Pallas kernels  177 us (97%)
  local copies, waits for them, and re-layouts  3.35 us (2%)
    pallas_call x1, Pallas kernels, per_device(): pl.pallas_call(kernel, out_shape=[jax.ShapeDtypeStruct((own, width), BF16...  177 us

profile of v3, /device:TPU:12, one launch (start us, length us, event | category | flops | bytes accessed | tf_op | source)
XLA Modules:
  0.0 181.5 jit_solution(13519727547632231614)
XLA Ops:
  0.6 177.5 %shard_map.176 = (bf16[128,4096]{1,0:T(8,128)(2,1)}, bf16[128,4096]{1,0:T(8,128)(2,1)}) custom-call(bf16[512,512]{1,0:T(8,128)(2,1)} %value.1, bf16[512,512]{1,0:T(8,128)(2,1)} %gate.1, f32[31,512]{1,0:T(8,128)} %taps.1, f32[1,512]{1,0:T(1,128)} %bitcast.13, f32[1,512]{1,0:T(1,128)} %bitcast.14, f32[1,512]{1,0:T(1,128)} %bitcast.15, f32[1,4096]{1,0:T(1,128)} %bitcast.12, ...), custom_call_target="tpu_custom_call" | custom-call | tf_op jit(solution)/shard_map/pallas_call | solution.py:609
  178.1 0.0 copy-start
  178.1 2.4 %copy.21 = bf16[128,4096]{1,0:T(8,128)(2,1)} copy(bf16[128,4096]{1,0:T(8,128)(2,1)} %get-tuple-element.4) | data formatting | bytes 2097152
  180.5 0.0 copy-done
  180.5 1.0 copy.22
Async XLA Ops:
  178.1 2.4 %copy-start = (bf16[128,4096]{1,0:T(8,128)(2,1)S(1)}, bf16[128,4096]{1,0:T(8,128)(2,1)}, u32[]{:S(2)}) copy-start(bf16[128,4096]{1,0:T(8,128)(2,1)} %get-tuple-element.5) | copy-start | bytes 3145732

commit v4 on v3

--- a/solution.py
+++ b/solution.py
@@ -8,6 +8,7 @@
 MESH = pl.DeviceIdType.MESH
 EPSILON = 1e-06
 CHUNKS = 4
+PIECES = 8
 TILE = 256
 STEP = 32
 UNIT = 16
@@ -45,7 +46,9 @@
     shared_gate,
     shared_up,
     shared_down,
-    mixer_ref,
+    mixer_own,
+    mixer_near,
+    mixer_far,
     out_ref,
     wbuf,
     opbuf,
@@ -72,6 +75,7 @@
     cols_st,
     choice,
     share_cols,
+    picks,
     froutes,
     load,
     put_sem,
@@ -182,6 +186,8 @@
     routes_far.start()
     down_far[0].start()
     down_far[1].start()
+    down_far[2].start()
+    down_far[3].start()
     gate_near.start()
     up_near.start()
     for c in range(CHUNKS):
@@ -242,7 +248,7 @@
         anywhere = anywhere + chosen
         for g in range(groups):
             choice[k, g] = chosen[:, g * batch : (g + 1) * batch].astype(BF16)
-    pick = anywhere.T.astype(BF16)
+    picks[...] = anywhere.T.astype(BF16)
 
     def going(g, to):
         return remote(box.at[g, to], rows.at[g, me], go_send.at[g, to], go_recv.at[g, me], {"ep": to})
@@ -252,19 +258,22 @@
             box.at[g, source], rows.at[g, source], go_send.at[g, source], go_recv.at[g, source], {"ep": source}
         )
 
-    for g in range(groups):
-        part = pick[g * batch : (g + 1) * batch]
-
+    def gather_rows(g):
         @pl.loop(0, tiles)
         def _(i):
             at = aligned(i, TILE)
+            part = picks[g * batch : (g + 1) * batch]
             box[g, :, :, at] = dot(part, tok[aligned(t, own), at]).astype(BF16).reshape(count, UNIT, TILE)
 
+        rows[g, me] = box[g, me]
+
+    def send_rows(g):
         @pl.loop(1, count)
         def _(j):
             going(g, lax.rem(me + j, count)).start()
 
-        rows[g, me] = box[g, me]
+    gather_rows(0)
+    send_rows(0)
 
     normalize(far_t)
     routes_far.wait()
@@ -293,6 +302,9 @@
     for g in range(groups):
         doubles[g].start()
         frows[g, me] = dup[g, me - base]
+
+    if groups > 1:
+        gather_rows(1)
 
     @pl.when(me < count - 1)
     def _():
@@ -357,12 +369,14 @@
             rows.at[g, source], frows.at[g, source], f_send.at[g, source], f_recv.at[g, source], far
         )
 
-    def forward_group(g):
-        @pl.loop(0, count - 2)
+    def forward_some(g, start, stop):
+        @pl.loop(start, stop)
         def _(j):
             came(g, outside(j)).wait_recv()
             forward(g, outside(j)).start()
 
+    def forward_group(g):
+        forward_some(g, 0, count - 2)
         came(g, partner).wait_recv()
 
     def far_ready(g):
@@ -417,10 +431,19 @@
     to_near = [
         remote(ns, nr.at[which], rs_near.at[which, 0], rs_near.at[which, 1], near) for which in range(2)
     ]
-    crossing = [
-        remote(kept.at[which, 1 - low], arr.at[which], rs_far.at[which, 0], rs_far.at[which, 1], far)
-        for which in range(2)
-    ]
+    piece = width // PIECES
+
+    def crossing(which, c, into):
+        return remote(
+            kept.at[which, 1 - low, :, pl.ds(c * piece, piece)],
+            into.at[:, pl.ds(c * piece, piece)],
+            rs_far.at[which, 0, c],
+            rs_far.at[which, 1, c],
+            far,
+        )
+
+    shared_cross = [crossing(0, c, arr) for c in range(PIECES)]
+    mixer_cross = [crossing(1, c, mixer_far) for c in range(PIECES)]
 
     def joined(which):
         to_near[which].wait_recv()
@@ -479,19 +502,14 @@
             if g:
                 total += total_out[:, at]
             if g == groups - 1:
-                arr[0, :, at] = (total + ended(0, at).astype(F32)).astype(BF16)
+                arr[:, at] = (total + ended(at).astype(F32)).astype(BF16)
             else:
                 total_out[:, at] = total
 
-    def ended(which, at):
+    def ended(at):
         return (
-            kept[which, low, :, at].astype(F32)
-            + nr[which, low, :, at].astype(F32)
-            + arr[which, :, at].astype(F32)
+            kept[0, low, :, at].astype(F32) + nr[0, low, :, at].astype(F32) + arr[:, at].astype(F32)
         ).astype(BF16)
-
-    def put(which, into):
-        return pltpu.make_async_copy(arr.at[which], into, put_sem.at[which])
 
     def normed():
         stat_far.wait()
@@ -514,9 +532,11 @@
 
     get_op = fetch(out_proj, opbuf, 5)
 
+    if groups > 1:
+        send_rows(1)
+    for g in range(2, groups):
+        gather_rows(g)
     forward_group(0)
-    down_far[2].start()
-    down_far[3].start()
     relay(0)
     relay(1)
     get_own_gate.wait()
@@ -528,52 +548,77 @@
     halves(0, hs, hidden)
     to_near[0].start()
     get_op.start()
-    far_part(0)
+    for g in range(2, groups):
+        send_rows(g)
+    relay(2)
     normed()
-    if groups > 1:
-        forward_group(1)
-        own_part(1)
     get_op.wait()
     to_near[0].wait_send()
     halves(1, act, act.shape[1])
     to_near[1].start()
     joined(0)
-    relay(2)
+    shared_cross[0].start()
+    far_part(0)
+    if groups > 1:
+        forward_group(1)
+        own_part(1)
     relay(3)
     get_down.wait()
     for c in range(CHUNKS):
         down_near[c].wait()
         down_on[c].wait()
     products(0)
+    joined(1)
+    keeps = [
+        pltpu.make_async_copy(part.at[1, low], into, put_sem.at[1 + i])
+        for i, (part, into) in enumerate(((kept, mixer_own), (nr, mixer_near)))
+    ]
+    for keep in keeps:
+        keep.start()
+
+    def finish_crossing():
+        for copy in shared_cross[2:] + mixer_cross:
+            copy.start()
+
+    half = (count - 2) // 2
     for g in range(1, groups):
-        if g > 1:
-            forward_group(g)
-            own_part(g)
-    joined(1)
-    for g in range(1, groups):
+        if g + 1 < groups:
+            forward_some(g + 1, 0, half)
         far_part(g)
-    crossing[0].start()
-    crossing[1].start()
-    for g in range(1, groups):
+        if g + 1 < groups:
+            forward_some(g + 1, half, count - 2)
+            came(g + 1, partner).wait_recv()
+            own_part(g + 1)
+            if g + 2 == groups:
+                shared_cross[1].start()
+        else:
+            finish_crossing()
         products(g)
+    if groups < 3:
+        shared_cross[1].start()
+    if groups == 1:
+        finish_crossing()
     for g in range(groups - 1):
         combine(g)
     for g in range(groups):
         doubles[g].wait_send()
     to_near[1].wait_send()
-    crossing[0].wait()
+    for copy in shared_cross:
+        copy.wait()
     combine(groups - 1)
-    put(0, out_ref).start()
-    crossing[1].wait()
-
-    @pl.loop(0, tiles)
-    def _(i):
-        at = aligned(i, TILE)
-        arr[1, :, at] = ended(1, at)
-
-    put(1, mixer_ref).start()
-    put(0, out_ref).wait()
-    put(1, mixer_ref).wait()
+    put = pltpu.make_async_copy(arr, out_ref, put_sem.at[0])
+    put.start()
+    for keep in keeps:
+        keep.wait()
+    put.wait()
+    for copy in mixer_cross:
+        copy.wait()
+
+
+def last_kernel(first, second, third, routed, mixer_ref, experts_ref):
+    total = first[...].astype(F32) + second[...].astype(F32) + third[...].astype(F32)
+    mixer_ref[...] = total.astype(BF16)
+    experts_ref[...] = routed[...]
 
 
 def per_device(
@@ -606,11 +651,11 @@
     vmem = pl.BlockSpec(memory_space=pltpu.VMEM)
     dma = pltpu.SemaphoreType.DMA
     mail = pltpu.VMEM((groups, ep_count, UNIT, width), BF16)
-    return pl.pallas_call(
+    *mixer_parts, experts_out = pl.pallas_call(
         kernel,
-        out_shape=[jax.ShapeDtypeStruct((own, width), BF16)] * 2,
+        out_shape=[jax.ShapeDtypeStruct((own, width), BF16)] * 4,
         in_specs=[vmem] * 9 + [anywhere] * 8,
-        out_specs=[anywhere, anywhere],
+        out_specs=[anywhere] * 4,
         scratch_shapes=[
             pltpu.VMEM((4, width, hidden), BF16),
             pltpu.VMEM((max(channels, hidden), width), BF16),
@@ -628,7 +673,7 @@
             pltpu.VMEM((2, own, width), BF16),
             pltpu.VMEM((2, 2, own, width), BF16),
             pltpu.VMEM((2, 2, own, width), BF16),
-            pltpu.VMEM((2, own, width), BF16),
+            pltpu.VMEM((own, width), BF16),
             pltpu.VMEM((2, 4 * own, hidden), F32),
             pltpu.VMEM((groups, 4, batch, hidden), BF16),
             pltpu.VMEM((groups, 2, batch, hidden), BF16),
@@ -637,9 +682,10 @@
             pltpu.VMEM((length, 128), F32),
             pltpu.VMEM((top_count, groups, own, batch), BF16),
             pltpu.VMEM((own, own), F32),
+            pltpu.VMEM((groups * batch, own), BF16),
             pltpu.VMEM((top_count, own), jnp.int32),
             dma((7,)),
-            dma((2,)),
+            dma((3,)),
             dma((4,)),
             dma((2,)),
             dma((4,)),
@@ -651,7 +697,7 @@
             dma((2, CHUNKS)),
             dma((2, CHUNKS)),
             dma((2, 2)),
-            dma((2, 2)),
+            dma((2, 2, PIECES)),
             dma((groups, ep_count)),
             dma((groups, ep_count)),
             dma((groups,)),
@@ -685,6 +731,14 @@
         shared_up,
         shared_down,
     )
+    blocks = pl.BlockSpec((own, width // CHUNKS), lambda i: (0, i))
+    return pl.pallas_call(
+        last_kernel,
+        grid=(CHUNKS,),
+        out_shape=[jax.ShapeDtypeStruct((own, width), BF16)] * 2,
+        in_specs=[blocks] * 4,
+        out_specs=[blocks] * 2,
+    )(*mixer_parts, experts_out)
 
 
 def solution(mesh):

time: 182 us -> 166 us (0.912); the launches traced: 181 us -> 163 us
  Pallas kernels: 177 us -> 162 us
  local copies, waits for them, and re-layouts: 3.35 us -> 0 us
    pallas_call x1, Pallas kernels: 177 us -> 158 us  [per_device(): pl.pallas_call(kernel, out_shape=[jax.ShapeDtypeStruct((own, width), BF16...]
    pallas_call x0 -> x1, Pallas kernels: none -> 4.16 us  [per_device(): pl.pallas_call(last_kernel, grid=(CHUNKS,), out_shape=[jax.ShapeDtypeStru...]
    unnamed x4 -> x0, local copies, waits for them, and re-layouts: 3.35 us -> none
where the time goes in v4:
time: 166 us; the launch traced here: 163 us
  Pallas kernels  162 us (98%)
    pallas_call x1, Pallas kernels, per_device(): pl.pallas_call(kernel, out_shape=[jax.ShapeDtypeStruct((own, width), BF16...  158 us
    pallas_call x1, Pallas kernels, per_device(): pl.pallas_call(last_kernel, grid=(CHUNKS,), out_shape=[jax.ShapeDtypeStru...  4.16 us

profile of v4, /device:TPU:12, one launch (start us, length us, event | category | flops | bytes accessed | tf_op | source)
XLA Modules:
  0.0 162.7 jit_solution(3478721262041976279)
XLA Ops:
  0.6 157.9 %shard_map.176 = (bf16[128,4096]{1,0:T(8,128)(2,1)}, bf16[128,4096]{1,0:T(8,128)(2,1)}, bf16[128,4096]{1,0:T(8,128)(2,1)}, bf16[128,4096]{1,0:T(8,128)(2,1)}) custom-call(bf16[512,512]{1,0:T(8,128)(2,1)} %value.1, bf16[512,512]{1,0:T(8,128)(2,1)} %gate.1, f32[31,512]{1,0:T(8,128)} %taps.1, f32[1,512]{1,0:T(1,128)} %bitcast.13, f32[1,512]{1,0:T(1,128)} %bitcast.14, ...), custom_call_target="tpu_custom_call" | custom-call | tf_op jit(solution)/shard_map/pallas_call | solution.py:654
  158.5 4.2 %shard_map.177 = (bf16[128,4096]{1,0:T(8,128)(2,1)}, bf16[128,4096]{1,0:T(8,128)(2,1)}) custom-call(bf16[128,4096]{1,0:T(8,128)(2,1)} %get-tuple-element.6.first, bf16[128,4096]{1,0:T(8,128)(2,1)} %get-tuple-element.7.second, bf16[128,4096]{1,0:T(8,128)(2,1)} %get-tuple-element.8.third, bf16[128,4096]{1,0:T(8,128)(2,1)} %get-tuple-element.9.routed), custom_call_target="tpu_custom_call" | custom-call | tf_op jit(solution)/shard_map/pallas_call | solution.py:735

commit v5 on v4

--- a/solution.py
+++ b/solution.py
@@ -9,9 +9,11 @@
 EPSILON = 1e-06
 CHUNKS = 4
 PIECES = 8
+EARLY = 2
 TILE = 256
 STEP = 32
 UNIT = 16
+HALF = 4
 RIM = 32
 F32, BF16 = jnp.float32, jnp.bfloat16
 
@@ -46,9 +48,7 @@
     shared_gate,
     shared_up,
     shared_down,
-    mixer_own,
-    mixer_near,
-    mixer_far,
+    mixer_ref,
     out_ref,
     wbuf,
     opbuf,
@@ -67,6 +67,7 @@
     kept,
     nr,
     arr,
+    mix,
     sacc,
     hid,
     hfar,
@@ -113,8 +114,8 @@
     near = {"tp": t + 1 - 2 * core}
     far = {"tp": lax.rem(t + 2, 4)}
     far_t = lax.rem(t + 2, 4)
-    base = (me // 2) * 2
-    partner = base + 1 - lax.rem(me, 2)
+    base = (me // HALF) * HALF
+    place_in = me - base
     hidden = hs.shape[1]
     tiles = width // TILE
 
@@ -187,7 +188,6 @@
     down_far[0].start()
     down_far[1].start()
     down_far[2].start()
-    down_far[3].start()
     gate_near.start()
     up_near.start()
     for c in range(CHUNKS):
@@ -277,31 +277,47 @@
 
     normalize(far_t)
     routes_far.wait()
-    spots = lax.broadcasted_iota(jnp.int32, (own, own), 1).astype(F32)
-    anywhere = jnp.zeros((own, own), F32)
+    spot_count = -(-groups * HALF * UNIT // 128) * 128
+    spots = lax.broadcasted_iota(jnp.int32, (own, spot_count), 1).astype(F32)
+    anywhere = jnp.zeros((own, spot_count), F32)
     first_of_pair = base.astype(F32)
     for r, place in placed(froutes[...]):
-        inside = (r - first_of_pair >= 0) & (r - first_of_pair <= 1)
-        spot = place + UNIT * (r - first_of_pair + jnp.floor(place * (1 / UNIT)))
+        inside = (r - first_of_pair >= 0) & (r - first_of_pair < HALF)
+        spot = place + UNIT * (r - first_of_pair + (HALF - 1) * jnp.floor(place * (1 / UNIT)))
         anywhere = anywhere + jnp.where(inside & (spots == spot), 1.0, 0.0)
-    pick = anywhere.T.astype(BF16)[: groups * 2 * UNIT]
+    pick = anywhere.T.astype(BF16)[: groups * HALF * UNIT]
 
     @pl.loop(0, tiles)
     def _(i):
         at = aligned(i, TILE)
         dup[:, :, :, at] = (
-            dot(pick, tok[aligned(far_t, own), at]).astype(BF16).reshape(groups, 2, UNIT, TILE)
-        )
-
-    doubles = [
-        remote(
-            dup.at[g, partner - base], frows.at[g, me], dup_send.at[g], dup_recv.at[g], {"ep": partner}
-        )
-        for g in range(groups)
-    ]
+            dot(pick, tok[aligned(far_t, own), at]).astype(BF16).reshape(groups, HALF, UNIT, TILE)
+        )
+
+    def double(g, j):
+        to = lax.rem(place_in + j, HALF)
+        return remote(
+            dup.at[g, to], frows.at[g, me], dup_send.at[g, to], dup_recv.at[g, place_in], {"ep": base + to}
+        )
+
+    def doubled(g, j):
+        source = lax.rem(place_in + j, HALF)
+        return remote(
+            dup.at[g, source],
+            frows.at[g, base + source],
+            dup_send.at[g, source],
+            dup_recv.at[g, source],
+            {"ep": base + source},
+        )
+
+    def send_doubles(g):
+        @pl.loop(1, HALF)
+        def _(j):
+            double(g, j).start()
+
     for g in range(groups):
-        doubles[g].start()
-        frows[g, me] = dup[g, me - base]
+        frows[g, me] = dup[g, place_in]
+    send_doubles(0)
 
     if groups > 1:
         gather_rows(1)
@@ -345,6 +361,7 @@
     stat[2] = stat[0] + stat[1]
     stat_far = remote(stat.at[2], stat.at[3], stat_sem.at[2], stat_sem.at[3], far)
     stat_far.start()
+    down_far[3].start()
     get_sg.wait()
     get_su.wait()
     sacc[...] = jnp.zeros_like(sacc)
@@ -362,7 +379,7 @@
     hs[...] = (silu(sacc[0]) * sacc[1]).astype(BF16)
 
     def outside(j):
-        return lax.rem(base + 2 + j, count)
+        return lax.rem(base + HALF + j, count)
 
     def forward(g, source):
         return remote(
@@ -375,14 +392,21 @@
             came(g, outside(j)).wait_recv()
             forward(g, outside(j)).start()
 
+    def near_came(g):
+        @pl.loop(1, HALF)
+        def _(j):
+            came(g, base + lax.rem(place_in + j, HALF)).wait_recv()
+
     def forward_group(g):
-        forward_some(g, 0, count - 2)
-        came(g, partner).wait_recv()
+        forward_some(g, 0, count - HALF)
+        near_came(g)
 
     def far_ready(g):
-        doubles[g].wait_recv()
-
-        @pl.loop(0, count - 2)
+        @pl.loop(1, HALF)
+        def _(j):
+            doubled(g, j).wait()
+
+        @pl.loop(0, count - HALF)
         def _(j):
             forward(g, outside(j)).wait()
 
@@ -443,7 +467,7 @@
         )
 
     shared_cross = [crossing(0, c, arr) for c in range(PIECES)]
-    mixer_cross = [crossing(1, c, mixer_far) for c in range(PIECES)]
+    mixer_cross = [crossing(1, c, mix) for c in range(PIECES)]
 
     def joined(which):
         to_near[which].wait_recv()
@@ -506,9 +530,11 @@
             else:
                 total_out[:, at] = total
 
-    def ended(at):
+    def ended(at, which=0, came_from=arr):
         return (
-            kept[0, low, :, at].astype(F32) + nr[0, low, :, at].astype(F32) + arr[:, at].astype(F32)
+            kept[which, low, :, at].astype(F32)
+            + nr[which, low, :, at].astype(F32)
+            + came_from[:, at].astype(F32)
         ).astype(BF16)
 
     def normed():
@@ -534,6 +560,7 @@
 
     if groups > 1:
         send_rows(1)
+        send_doubles(1)
     for g in range(2, groups):
         gather_rows(g)
     forward_group(0)
@@ -544,12 +571,13 @@
     gate_near.wait()
     up_near.wait()
     own_part(0)
+    for g in range(2, groups):
+        send_rows(g)
+        send_doubles(g)
     get_sd.wait()
     halves(0, hs, hidden)
     to_near[0].start()
     get_op.start()
-    for g in range(2, groups):
-        send_rows(g)
     relay(2)
     normed()
     get_op.wait()
@@ -569,56 +597,45 @@
         down_on[c].wait()
     products(0)
     joined(1)
-    keeps = [
-        pltpu.make_async_copy(part.at[1, low], into, put_sem.at[1 + i])
-        for i, (part, into) in enumerate(((kept, mixer_own), (nr, mixer_near)))
-    ]
-    for keep in keeps:
-        keep.start()
-
     def finish_crossing():
-        for copy in shared_cross[2:] + mixer_cross:
+        for copy in shared_cross[EARLY + 1 :] + mixer_cross:
             copy.start()
 
-    half = (count - 2) // 2
     for g in range(1, groups):
-        if g + 1 < groups:
-            forward_some(g + 1, 0, half)
+        if g + 2 == groups:
+            shared_cross[1].start()
         far_part(g)
         if g + 1 < groups:
-            forward_some(g + 1, half, count - 2)
-            came(g + 1, partner).wait_recv()
+            forward_group(g + 1)
+            if g + 2 == groups:
+                shared_cross[EARLY].start()
             own_part(g + 1)
-            if g + 2 == groups:
-                shared_cross[1].start()
         else:
             finish_crossing()
         products(g)
     if groups < 3:
-        shared_cross[1].start()
+        for copy in shared_cross[1 : EARLY + 1]:
+            copy.start()
     if groups == 1:
         finish_crossing()
     for g in range(groups - 1):
         combine(g)
-    for g in range(groups):
-        doubles[g].wait_send()
     to_near[1].wait_send()
-    for copy in shared_cross:
+    for copy in shared_cross + mixer_cross:
         copy.wait()
+
+    @pl.loop(0, tiles)
+    def _(i):
+        at = aligned(i, TILE)
+        mix[:, at] = ended(at, 1, mix)
+
+    put_mixer = pltpu.make_async_copy(mix, mixer_ref, put_sem.at[1])
+    put_mixer.start()
     combine(groups - 1)
     put = pltpu.make_async_copy(arr, out_ref, put_sem.at[0])
     put.start()
-    for keep in keeps:
-        keep.wait()
+    put_mixer.wait()
     put.wait()
-    for copy in mixer_cross:
-        copy.wait()
-
-
-def last_kernel(first, second, third, routed, mixer_ref, experts_ref):
-    total = first[...].astype(F32) + second[...].astype(F32) + third[...].astype(F32)
-    mixer_ref[...] = total.astype(BF16)
-    experts_ref[...] = routed[...]
 
 
 def per_device(
@@ -651,11 +668,11 @@
     vmem = pl.BlockSpec(memory_space=pltpu.VMEM)
     dma = pltpu.SemaphoreType.DMA
     mail = pltpu.VMEM((groups, ep_count, UNIT, width), BF16)
-    *mixer_parts, experts_out = pl.pallas_call(
+    return pl.pallas_call(
         kernel,
-        out_shape=[jax.ShapeDtypeStruct((own, width), BF16)] * 4,
+        out_shape=[jax.ShapeDtypeStruct((own, width), BF16)] * 2,
         in_specs=[vmem] * 9 + [anywhere] * 8,
-        out_specs=[anywhere] * 4,
+        out_specs=[anywhere] * 2,
         scratch_shapes=[
             pltpu.VMEM((4, width, hidden), BF16),
             pltpu.VMEM((max(channels, hidden), width), BF16),
@@ -663,7 +680,7 @@
             pltpu.VMEM((3, hidden, width), BF16),
             pltpu.VMEM((4 * own, width), BF16),
             mail,
-            pltpu.VMEM((groups, 2, UNIT, width), BF16),
+            pltpu.VMEM((groups, HALF, UNIT, width), BF16),
             mail,
             mail,
             mail,
@@ -673,6 +690,7 @@
             pltpu.VMEM((2, own, width), BF16),
             pltpu.VMEM((2, 2, own, width), BF16),
             pltpu.VMEM((2, 2, own, width), BF16),
+            pltpu.VMEM((own, width), BF16),
             pltpu.VMEM((own, width), BF16),
             pltpu.VMEM((2, 4 * own, hidden), F32),
             pltpu.VMEM((groups, 4, batch, hidden), BF16),
@@ -685,7 +703,7 @@
             pltpu.VMEM((groups * batch, own), BF16),
             pltpu.VMEM((top_count, own), jnp.int32),
             dma((7,)),
-            dma((3,)),
+            dma((2,)),
             dma((4,)),
             dma((2,)),
             dma((4,)),
@@ -700,8 +718,8 @@
             dma((2, 2, PIECES)),
             dma((groups, ep_count)),
             dma((groups, ep_count)),
-            dma((groups,)),
-            dma((groups,)),
+            dma((groups, HALF)),
+            dma((groups, HALF)),
             dma((groups, ep_count)),
             dma((groups, ep_count)),
             dma((groups, 2)),
@@ -731,14 +749,6 @@
         shared_up,
         shared_down,
     )
-    blocks = pl.BlockSpec((own, width // CHUNKS), lambda i: (0, i))
-    return pl.pallas_call(
-        last_kernel,
-        grid=(CHUNKS,),
-        out_shape=[jax.ShapeDtypeStruct((own, width), BF16)] * 2,
-        in_specs=[blocks] * 4,
-        out_specs=[blocks] * 2,
-    )(*mixer_parts, experts_out)
 
 
 def solution(mesh):

time: 166 us -> 157 us (0.946); the launches traced: 163 us -> 156 us
  Pallas kernels: 162 us -> 152 us
  local copies, waits for them, and re-layouts: 0 us -> 3.35 us
    pallas_call x1, Pallas kernels: 158 us -> 152 us  [per_device(): pl.pallas_call(kernel, out_shape=[jax.ShapeDtypeStruct((own, width), BF16...]
    pallas_call x1 -> x0, Pallas kernels: 4.16 us -> none  [per_device(): pl.pallas_call(last_kernel, grid=(CHUNKS,), out_shape=[jax.ShapeDtypeStru...]
    unnamed x0 -> x4, local copies, waits for them, and re-layouts: none -> 3.35 us
where the time goes in v5:
time: 157 us; the launch traced here: 156 us
  Pallas kernels  152 us (97%)
  local copies, waits for them, and re-layouts  3.35 us (2%)
    pallas_call x1, Pallas kernels, per_device(): pl.pallas_call(kernel, out_shape=[jax.ShapeDtypeStruct((own, width), BF16...  152 us
    unnamed x4, local copies, waits for them, and re-layouts  3.35 us

profile of v5, /device:TPU:12, one launch (start us, length us, event | category | flops | bytes accessed | tf_op | source)
XLA Modules:
  0.0 156.4 jit_solution(18031273227101519960)
XLA Ops:
  0.6 152.4 %shard_map.176 = (bf16[128,4096]{1,0:T(8,128)(2,1)}, bf16[128,4096]{1,0:T(8,128)(2,1)}) custom-call(bf16[512,512]{1,0:T(8,128)(2,1)} %value.1, bf16[512,512]{1,0:T(8,128)(2,1)} %gate.1, f32[31,512]{1,0:T(8,128)} %taps.1, f32[1,512]{1,0:T(1,128)} %bitcast.13, f32[1,512]{1,0:T(1,128)} %bitcast.14, f32[1,512]{1,0:T(1,128)} %bitcast.15, f32[1,4096]{1,0:T(1,128)} %bitcast.12, ...), custom_call_target="tpu_custom_call" | custom-call | tf_op jit(solution)/shard_map/pallas_call | solution.py:671
  153.1 0.0 copy-start
  153.1 2.4 %copy.21 = bf16[128,4096]{1,0:T(8,128)(2,1)} copy(bf16[128,4096]{1,0:T(8,128)(2,1)} %get-tuple-element.4) | data formatting | bytes 2097152
  155.4 0.0 copy-done
  155.4 1.0 copy.22
Async XLA Ops:
  153.1 2.4 %copy-start = (bf16[128,4096]{1,0:T(8,128)(2,1)S(1)}, bf16[128,4096]{1,0:T(8,128)(2,1)}, u32[]{:S(2)}) copy-start(bf16[128,4096]{1,0:T(8,128)(2,1)} %get-tuple-element.5) | copy-start | bytes 3145732

commit v6 on v5

--- a/solution.py
+++ b/solution.py
@@ -9,7 +9,7 @@
 EPSILON = 1e-06
 CHUNKS = 4
 PIECES = 8
-EARLY = 2
+EARLY = 3
 TILE = 256
 STEP = 32
 UNIT = 16
@@ -31,8 +31,8 @@
 
 
 def kernel(
-    value,
-    gate,
+    value_in,
+    gate_in,
     taps,
     bias,
     ln_gain,
@@ -50,6 +50,8 @@
     shared_down,
     mixer_ref,
     out_ref,
+    value,
+    gate,
     wbuf,
     opbuf,
     dbuf,
@@ -143,6 +145,10 @@
     def tokens_load(b):
         return pltpu.make_async_copy(tokens.at[aligned(b, own)], tok.at[aligned(b, own)], tok_load.at[b])
 
+    get_value = fetch(value_in, value, 7)
+    get_gate = fetch(gate_in, gate, 8)
+    get_value.start()
+    get_gate.start()
     tokens_load(t).start()
     tokens_load(far_t).start()
     get_sg = fetch(shared_gate, wbuf.at[0], 0)
@@ -193,6 +199,9 @@
     for c in range(CHUNKS):
         down_near[c].start()
 
+    get_value.wait()
+    get_gate.wait()
+
     @pl.loop(0, length // STEP)
     def _(i):
         at = aligned(i, STEP)
@@ -251,11 +260,11 @@
     picks[...] = anywhere.T.astype(BF16)
 
     def going(g, to):
-        return remote(box.at[g, to], rows.at[g, me], go_send.at[g, to], go_recv.at[g, me], {"ep": to})
+        return remote(box.at[g, to], rows.at[g, me], go_send.at[g], go_recv.at[g, me], {"ep": to})
 
     def came(g, source):
         return remote(
-            box.at[g, source], rows.at[g, source], go_send.at[g, source], go_recv.at[g, source], {"ep": source}
+            box.at[g, source], rows.at[g, source], go_send.at[g], go_recv.at[g, source], {"ep": source}
         )
 
     def gather_rows(g):
@@ -381,16 +390,15 @@
     def outside(j):
         return lax.rem(base + HALF + j, count)
 
-    def forward(g, source):
-        return remote(
-            rows.at[g, source], frows.at[g, source], f_send.at[g, source], f_recv.at[g, source], far
-        )
+    def forward(g, j):
+        source = outside(j)
+        return remote(rows.at[g, source], frows.at[g, source], f_send.at[g, j], f_recv.at[g, j], far)
 
     def forward_some(g, start, stop):
         @pl.loop(start, stop)
         def _(j):
             came(g, outside(j)).wait_recv()
-            forward(g, outside(j)).start()
+            forward(g, j).start()
 
     def near_came(g):
         @pl.loop(1, HALF)
@@ -408,7 +416,7 @@
 
         @pl.loop(0, count - HALF)
         def _(j):
-            forward(g, outside(j)).wait()
+            forward(g, j).wait()
 
     def ffn(source, g, slot):
         lhs = source.at[g]
@@ -480,12 +488,12 @@
             ).astype(BF16)
 
     def back(g, to):
-        return remote(box.at[g, to], ret.at[g, me], ret_send.at[g, to], ret_recv.at[g, me], {"ep": to})
+        return remote(box.at[g, to], ret.at[g, me], ret_send.at[g], ret_recv.at[g], {"ep": to})
 
     def products(g):
-        @pl.loop(1, count)
-        def _(j):
-            came(g, lax.rem(me + j, count)).wait_send()
+        others = pl.ds(0, count - 1)
+        after = {"ep": lax.rem(me + 1, count)}
+        remote(box.at[g, others], rows.at[g, others], go_send.at[g], go_recv.at[g, 0], after).wait_send()
 
         for n in range(2):
             hidden_far[g][n].wait()
@@ -505,19 +513,11 @@
         ret[g, me] = box[g, me]
 
     def combine(g):
-        @pl.loop(1, count)
-        def _(j):
-            source = lax.rem(me + j, count)
-            remote(
-                box.at[g, source],
-                ret.at[g, source],
-                ret_send.at[g, source],
-                ret_recv.at[g, source],
-                {"ep": source},
-            ).wait()
-
-        @pl.loop(0, tiles)
-        def _(i):
+        others = pl.ds(0, count - 1)
+        after = {"ep": lax.rem(me + 1, count)}
+        remote(box.at[g, others], ret.at[g, others], ret_send.at[g], ret_recv.at[g], after).wait()
+
+        def tile(i):
             at = aligned(i, TILE)
             back_rows = ret[g, :, :, at].reshape(batch, TILE)
             total = jnp.zeros((own, TILE), F32)
@@ -529,6 +529,16 @@
                 arr[:, at] = (total + ended(at).astype(F32)).astype(BF16)
             else:
                 total_out[:, at] = total
+
+        if g < groups - 1:
+            pl.loop(0, tiles)(tile)
+        else:
+            for c in range(CHUNKS):
+                pl.loop(c * tiles // CHUNKS, (c + 1) * tiles // CHUNKS)(tile)
+                put(c).start()
+
+    def put(c):
+        return pltpu.make_async_copy(arr.at[:, cols(c)], out_ref.at[:, cols(c)], put_sem.at[c])
 
     def ended(at, which=0, came_from=arr):
         return (
@@ -606,9 +616,10 @@
             shared_cross[1].start()
         far_part(g)
         if g + 1 < groups:
+            if g + 2 == groups:
+                for copy in shared_cross[2 : EARLY + 1]:
+                    copy.start()
             forward_group(g + 1)
-            if g + 2 == groups:
-                shared_cross[EARLY].start()
             own_part(g + 1)
         else:
             finish_crossing()
@@ -629,13 +640,12 @@
         at = aligned(i, TILE)
         mix[:, at] = ended(at, 1, mix)
 
-    put_mixer = pltpu.make_async_copy(mix, mixer_ref, put_sem.at[1])
+    put_mixer = pltpu.make_async_copy(mix, mixer_ref, put_sem.at[CHUNKS])
     put_mixer.start()
     combine(groups - 1)
-    put = pltpu.make_async_copy(arr, out_ref, put_sem.at[0])
-    put.start()
     put_mixer.wait()
-    put.wait()
+    for c in range(CHUNKS):
+        put(c).wait()
 
 
 def per_device(
@@ -671,9 +681,11 @@
     return pl.pallas_call(
         kernel,
         out_shape=[jax.ShapeDtypeStruct((own, width), BF16)] * 2,
-        in_specs=[vmem] * 9 + [anywhere] * 8,
+        in_specs=[anywhere] * 2 + [vmem] * 7 + [anywhere] * 8,
         out_specs=[anywhere] * 2,
         scratch_shapes=[
+            pltpu.VMEM((length, channels), BF16),
+            pltpu.VMEM((length, channels), BF16),
             pltpu.VMEM((4, width, hidden), BF16),
             pltpu.VMEM((max(channels, hidden), width), BF16),
             pltpu.VMEM((hidden, width), BF16),
@@ -702,8 +714,8 @@
             pltpu.VMEM((own, own), F32),
             pltpu.VMEM((groups * batch, own), BF16),
             pltpu.VMEM((top_count, own), jnp.int32),
-            dma((7,)),
-            dma((2,)),
+            dma((9,)),
+            dma((CHUNKS + 1,)),
             dma((4,)),
             dma((2,)),
             dma((4,)),
@@ -716,16 +728,16 @@
             dma((2, CHUNKS)),
             dma((2, 2)),
             dma((2, 2, PIECES)),
-            dma((groups, ep_count)),
+            dma((groups,)),
             dma((groups, ep_count)),
             dma((groups, HALF)),
             dma((groups, HALF)),
-            dma((groups, ep_count)),
-            dma((groups, ep_count)),
+            dma((groups, ep_count - HALF)),
+            dma((groups, ep_count - HALF)),
             dma((groups, 2)),
             dma((groups, 2)),
-            dma((groups, ep_count)),
-            dma((groups, ep_count)),
+            dma((groups,)),
+            dma((groups,)),
         ],
         compiler_params=pltpu.CompilerParams(
             collective_id=0, has_side_effects=True, vmem_limit_bytes=67043328

time: 157 us -> 155 us (0.987)
  no operation moved by 1% of the time
where the time goes in v6:
time: 155 us
  Pallas kernels  151 us (97%)
  local copies, waits for them, and re-layouts  3.35 us (2%)
    pallas_call x1, Pallas kernels, per_device(): pl.pallas_call(kernel, out_shape=[jax.ShapeDtypeStruct((own, width), BF16...  151 us
    unnamed x4, local copies, waits for them, and re-layouts  3.35 us

profile of v6, /device:TPU:12, one launch (start us, length us, event | category | flops | bytes accessed | tf_op | source)
XLA Modules:
  0.0 155.0 jit_solution(12776848623793139441)
XLA Ops:
  0.6 151.0 %shard_map.176 = (bf16[128,4096]{1,0:T(8,128)(2,1)}, bf16[128,4096]{1,0:T(8,128)(2,1)}) custom-call(bf16[512,512]{1,0:T(8,128)(2,1)} %value_in.1, bf16[512,512]{1,0:T(8,128)(2,1)} %gate_in.1, f32[31,512]{1,0:T(8,128)} %taps.1, f32[1,512]{1,0:T(1,128)} %bitcast.13, f32[1,512]{1,0:T(1,128)} %bitcast.14, f32[1,512]{1,0:T(1,128)} %bitcast.15, ...), custom_call_target="tpu_custom_call" | custom-call | tf_op jit(solution)/shard_map/pallas_call | solution.py:681
  151.6 0.0 copy-start
  151.6 2.4 %copy.21 = bf16[128,4096]{1,0:T(8,128)(2,1)} copy(bf16[128,4096]{1,0:T(8,128)(2,1)} %get-tuple-element.4) | data formatting | bytes 2097152
  154.0 0.0 copy-done
  154.0 1.0 copy.22
Async XLA Ops:
  151.6 2.4 %copy-start = (bf16[128,4096]{1,0:T(8,128)(2,1)S(1)}, bf16[128,4096]{1,0:T(8,128)(2,1)}, u32[]{:S(2)}) copy-start(bf16[128,4096]{1,0:T(8,128)(2,1)} %get-tuple-element.5) | copy-start | bytes 3145732
